TPU v7x, 128 devices: a whole 4x4x4 slice. The times are simulated.
128 devices in a mesh: sp: 32 (over z, y, core), tp: 4 (over x).
Axes of the slice: x: 4, y: 4, z: 4, core: 2. Of those that a mesh axis runs over, the one named last changes fastest.
Arguments:
- queries: bfloat16 [16384, 1024], P('sp', 'tp'), may hold values from -6 to 6
- key_heads: bfloat16 [16384, 512], P('sp', 'tp'), may hold values from -6 to 6
- value_heads: bfloat16 [16384, 512], P('sp', 'tp'), may hold values from -70 to 70
- documents: int32 [16384], P('sp'), may hold values from 0 to 8, never falling along the last dimension, each value on 1 to 10240 neighbouring positions
- query_gain: float32 [128], replicated, may hold values from 0.1 to 8
- key_gain: float32 [128], replicated, may hold values from 0.1 to 8
- out_gain: float32 [1024], replicated, may hold values from 0.1 to 1.9
- out_proj: bfloat16 [1024, 2048], replicated, may hold values from -0.1875 to 0.1875
- residual: bfloat16 [16384, 2048], P(('sp', 'tp')), may hold values from -6 to 6
- mid_gain: float32 [2048], replicated, may hold values from 0.1 to 1.9
- mid_bias: float32 [2048], replicated, may hold values from -1.5 to 1.5
- routes: int32 [16384, 2], P(('sp', 'tp')), may hold values from 0 to 127, all different within a row; in each aligned block of 128 rows (0 to 127, 128 to 255, ...) at most 4 rows name the same one
- route_weights: float32 [16384, 2], P(('sp', 'tp')), may hold values from 0.2 to 2
- expert_gate: bfloat16 [128, 2048, 512], P(('sp', 'tp')), may hold values from -0.125 to 0.125
- expert_up: bfloat16 [128, 2048, 512], P(('sp', 'tp')), may hold values from -0.125 to 0.125
- expert_down: bfloat16 [128, 512, 2048], P(('sp', 'tp')), may hold values from -0.25 to 0.25
- final_gain: float32 [2048], replicated, may hold values from 0.1 to 1.9
- final_bias: float32 [2048], replicated, may hold values from -1.5 to 1.5
Outputs:
- layer_out: bfloat16 [16384, 2048], P(('sp', 'tp'))
Inputs may be any that keep to these rules, and one draw needn't show every extreme that they name: `documents`: never falls along the sequence; each document holds 1 to 10240 positions and one holds exactly 10240. `routes`: each row names 2 different experts; among the rows of one device (aligned blocks of 128 rows) no expert is named more than 4 times, and exactly 4 times in some block.
All inputs are finite; a program needn't handle non-finite values.
Results may differ from a plain program's by a relative error of at most 0.014.
The roundings to bfloat16 on the way count: a program that leaves them out, or rounds other values in their place, can miss the bound.
Values may be sent and summed in bfloat16 or wider, within the bound.
No kernel may reach another device: no remote copies, remote signals or barrier semaphores. Data moves between devices by JAX's collectives and lax.ppermute only.
A program may use at most 128 MiB of HBM per device.

v0:
```python
import math

import jax
import jax.numpy as jnp
from jax import lax
from jax.sharding import PartitionSpec as P

HEAD = 128
GRID = 64


eps_norm = 1e-06
alpha_mix = 8.0**0.25
theta_base = 10000.0


def sent_together(arrays, axis, dim, along):
    widths = [a.shape[along] for a in arrays]
    both = jnp.concatenate(arrays, axis=along)
    filled = lax.all_gather(both, axis, axis=dim, tiled=True)
    return tuple(jnp.split(filled, [sum(widths[:k]) for k in range(1, len(widths))], axis=along))


def split_up(shard, dim, length):
    before, after = (shard.shape[:dim], shard.shape[dim + 1 :])
    return jnp.moveaxis(shard.reshape(*before, length, -1, *after), dim, 0)


def sent_and_summed(shard, axis, dim):
    tiles = split_up(shard, dim, lax.axis_size(axis))
    arrived = lax.all_to_all(tiles, axis, split_axis=0, concat_axis=0, tiled=True)
    return arrived.sum(axis=0)


def rotary_tables(row_total, offset):
    positions = offset + jnp.arange(row_total, dtype=jnp.int32)
    grid_row = (positions // GRID).astype(jnp.float32)
    grid_col = (positions % GRID).astype(jnp.float32)
    pair_count = HEAD // 4
    inv_freq = theta_base ** (-jnp.arange(pair_count, dtype=jnp.float32) / pair_count)
    angles = jnp.concatenate(
        [grid_row[:, None] * inv_freq[None, :], grid_col[:, None] * inv_freq[None, :]], axis=1
    )
    return (jnp.cos(angles), jnp.sin(angles))


def normed_rotated(heads_in, gain_vec, cosine_table, sine_table):
    values = heads_in.astype(jnp.float32)
    inv_rms = lax.rsqrt(jnp.mean(values * values, axis=-1, keepdims=True) + eps_norm)
    values = values * inv_rms * gain_vec
    half_dim = HEAD // 2
    first_half = values[..., :half_dim]
    second_half = values[..., half_dim:]
    cosine_part = cosine_table[:, None, :]
    sine_part = sine_table[:, None, :]
    turned = jnp.concatenate(
        [
            first_half * cosine_part - second_half * sine_part,
            second_half * cosine_part + first_half * sine_part,
        ],
        axis=-1,
    )
    return turned.astype(jnp.bfloat16)


def layer_norm(stream, gain_vec, bias_vec):
    center = jnp.mean(stream, axis=-1, keepdims=True)
    spread = jnp.mean(jnp.square(stream - center), axis=-1, keepdims=True)
    return (stream - center) * lax.rsqrt(spread + eps_norm) * gain_vec + bias_vec


def per_device(
    queries,
    key_heads,
    value_heads,
    documents,
    query_gain,
    key_gain,
    out_gain,
    out_proj,
    residual,
    mid_gain,
    mid_bias,
    routes,
    route_weights,
    expert_gate,
    expert_up,
    expert_down,
    final_gain,
    final_bias,
):
    tok_rows = queries.shape[0]
    query_local = queries.shape[1] // HEAD
    key_local = key_heads.shape[1] // HEAD
    grouped = query_local // key_local
    offset = lax.axis_index("sp") * tok_rows
    cosine_table, sine_table = rotary_tables(tok_rows, offset)
    query_rot = normed_rotated(
        queries.reshape(tok_rows, query_local, HEAD), query_gain, cosine_table, sine_table
    ).reshape(tok_rows, key_local, grouped, HEAD)
    key_rot = normed_rotated(
        key_heads.reshape(tok_rows, key_local, HEAD), key_gain, cosine_table, sine_table
    ).reshape(tok_rows, key_local * HEAD)
    first_doc = documents[0]
    last_doc = documents[tok_rows - 1]
    start_state = (
        jnp.full((key_local, grouped, tok_rows), -1e30, jnp.float32),
        jnp.zeros((key_local, grouped, tok_rows), jnp.float32),
        jnp.zeros((key_local, grouped, tok_rows, HEAD), jnp.float32),
    )
    key_part, value_part, doc_part = (
        *sent_together((key_rot, value_heads), "sp", 0, 1),
        lax.all_gather(documents, "sp", axis=0, tiled=True),
    )
    piece_rows = key_part.shape[0]
    block_rows = math.gcd(piece_rows, 512)
    block_count = piece_rows // block_rows
    blocks = (
        key_part.reshape(block_count, block_rows, key_local, HEAD),
        value_part.reshape(block_count, block_rows, key_local, HEAD),
        doc_part.reshape(block_count, block_rows),
    )

    def advance(running, block_set):
        key_block, value_block, doc_block = block_set
        running_max, running_total, running_sum = running
        scores = jnp.einsum(
            "qkgd,tkd->kgqt", query_rot, key_block, preferred_element_type=jnp.float32
        ) * HEAD ** (-0.5)
        allowed = (documents[:, None] == doc_block[None, :])[None, None]
        scores = jnp.where(allowed, scores, -1e30)
        new_max = jnp.maximum(running_max, jnp.max(scores, axis=-1))
        weights = jnp.where(allowed, jnp.exp(scores - new_max[..., None]), 0.0)
        rescale = jnp.exp(running_max - new_max)
        new_total = running_total * rescale + jnp.sum(weights, axis=-1)
        new_sum = running_sum * rescale[..., None] + jnp.einsum(
            "kgqt,tkd->kgqd",
            weights.astype(jnp.bfloat16),
            value_block,
            preferred_element_type=jnp.float32,
        )
        return ((new_max, new_total, new_sum), None)

    def process(running):
        result, unused = lax.scan(advance, running, blocks)
        return result

    touches = (doc_part[0] <= last_doc) & (doc_part[piece_rows - 1] >= first_doc)
    final_max, final_total, final_sum = lax.cond(
        touches, process, lambda running: running, start_state
    )
    attention = jnp.transpose(final_sum / final_total[..., None], (2, 0, 1, 3))
    attention = attention.reshape(tok_rows, query_local * HEAD).astype(jnp.bfloat16)
    local_width = query_local * HEAD
    attn_float = attention.astype(jnp.float32)
    squares = sent_and_summed(jnp.sum(attn_float * attn_float, axis=1), "tp", 0)
    mean_square = squares / out_gain.shape[0]
    own_gain = lax.dynamic_slice_in_dim(
        out_gain, lax.axis_index("tp") * local_width, local_width, 0
    )
    own_rows = lax.dynamic_slice_in_dim(
        out_proj, lax.axis_index("tp") * local_width, local_width, 0
    )
    scaled = (attn_float * own_gain).astype(jnp.bfloat16)
    projected = lax.psum_scatter(
        jnp.dot(scaled, own_rows, preferred_element_type=jnp.float32).astype(jnp.bfloat16),
        "tp",
        scatter_dimension=0,
        tiled=True,
    ).astype(jnp.float32)
    projected = projected * lax.rsqrt(mean_square + eps_norm)[:, None]
    middle = layer_norm(
        alpha_mix * residual.astype(jnp.float32) + projected, mid_gain, mid_bias
    ).astype(jnp.bfloat16)
    out_rows = middle.shape[0]
    model_width = middle.shape[1]
    top_count = routes.shape[1]
    local_experts = expert_gate.shape[0]
    sp_size = lax.axis_size("sp")
    tp_size = lax.axis_size("tp")
    expert_total = local_experts * sp_size * tp_size
    capacity = 2 * out_rows * top_count // expert_total
    flat_routes = routes.reshape(-1)
    one_hot = (flat_routes[:, None] == jnp.arange(expert_total, dtype=jnp.int32)[None, :]).astype(
        jnp.int32
    )
    rank_in = jnp.sum((jnp.cumsum(one_hot, axis=0) - one_hot) * one_hot, axis=1)
    target = flat_routes * capacity + rank_in
    outbound = (
        jnp.zeros((expert_total * capacity, model_width), jnp.bfloat16)
        .at[target]
        .set(jnp.repeat(middle, top_count, axis=0))
    )
    arrived = lax.all_to_all(
        outbound.reshape(expert_total, capacity, model_width),
        ("sp", "tp"),
        split_axis=0,
        concat_axis=0,
        tiled=True,
    )
    item_count = arrived.shape[-2]
    grouped_rows = arrived.reshape(-1, local_experts, item_count, model_width)
    gate_part = jnp.einsum(
        "sekd,edf->sekf", grouped_rows, expert_gate, preferred_element_type=jnp.float32
    )
    up_part = jnp.einsum(
        "sekd,edf->sekf", grouped_rows, expert_up, preferred_element_type=jnp.float32
    )
    hidden = (jax.nn.silu(gate_part) * up_part).astype(jnp.bfloat16)
    served = jnp.einsum("sekf,efd->sekd", hidden, expert_down, preferred_element_type=jnp.float32)
    returned = lax.all_to_all(
        served.astype(jnp.bfloat16).reshape(arrived.shape),
        ("sp", "tp"),
        split_axis=0,
        concat_axis=0,
        tiled=True,
    )
    picked = returned.reshape(expert_total * capacity, model_width)[target]
    picked = picked.astype(jnp.float32).reshape(out_rows, top_count, model_width)
    routed = jnp.sum(picked * route_weights[:, :, None], axis=1)
    return layer_norm(
        alpha_mix * middle.astype(jnp.float32) + routed, final_gain, final_bias
    ).astype(jnp.bfloat16)


def solution(mesh):
    return jax.shard_map(
        per_device,
        mesh=mesh,
        in_specs=(
            P("sp", "tp"),
            P("sp", "tp"),
            P("sp", "tp"),
            P("sp"),
            P(),
            P(),
            P(),
            P(),
            P(("sp", "tp"), None),
            P(),
            P(),
            P(("sp", "tp"), None),
            P(("sp", "tp"), None),
            P(("sp", "tp"), None, None),
            P(("sp", "tp"), None, None),
            P(("sp", "tp"), None, None),
            P(),
            P(),
        ),
        out_specs=P(("sp", "tp"), None),
        check_vma=False,
    )
```

profile of v0, /device:TPU:1, one launch (start us, length us, event | category | flops | bytes accessed | tf_op | source)
XLA Modules:
  0.0 485.2 jit_solution(16943709737238043858)
XLA Ops:
  10.6 27.1 %all-gather = s32[32,1,512]{2,1,0:T(1,128)S(1)} all-gather(s32[1,1,512]{2,1,0:T(1,128)S(1)} %bitcast.177), channel_id=1, replica_groups=mesh['sp'=32,'tp'=4] {'sp'}, dimensions={0}, use_global_device_ids=true | all-gather | bytes 67584 | tf_op jit(solution)/shard_map/all_gather | solution.py:113
  42.7 24.3 %all-gather.3.cloned.1.call-done = bf16[16384,256]{1,0:T(8,128)(2,1)} async-done(((bf16[512,256]{1,0:T(8,128)(2,1)}), bf16[16384,256]{1,0:T(8,128)(2,1)}) %all-gather.3.cloned.1.call-update) | async-done | bytes 8388624 | tf_op jit(solution)/shard_map/all_gather | solution.py:20
  67.0 251.5 %conditional.1 = (f32[1,2,512]{2,1,0:T(2,128)}, f32[1,2,512,128]{2,3,1,0:T(8,128)S(1)}) conditional(s32[]{:T(128)} %bitcast.4, () %tuple.17, (bf16[16384,256]{1,0:T(8,128)(2,1)}, s32[16384]{0:T(1024)S(1)}, s32[512]{0:T(512)S(1)}, bf16[512,1,2,128]{0,3,2,1:T(8,128)(2,1)S(1)}) %tuple.68), branch_computations={%region_2.3_spmd, %region_3.8_spmd} | conditional | flops 275912704 | bytes 37954852 | solution.py:149
  67.0 5.7 %fusion.95 = (bf16[16384,128]{1,0:T(8,128)(2,1)}, bf16[16384,128]{1,0:T(8,128)(2,1)}) fusion(bf16[16384,256]{1,0:T(8,128)(2,1)} %get-tuple-element.67), kind=kLoop, calls=%fused_computation.131 | loop fusion | bytes 16777216 | tf_op jit(solution)/shard_map/split | solution.py:21
  73.0 243.5 %while.14 = (s32[]{:T(128)}, f32[1,2,512]{2,1,0:T(2,128)S(1)}, f32[1,2,512]{2,1,0:T(2,128)}, f32[1,2,512,128]{3,2,1,0:T(8,128)S(1)}, s32[512]{0:T(512)S(1)}, /*i...) while((s32[]{:T(128)}, f32[1,2,512]{2,1,0:T(2,128)S(1)}, ...), condition=%wide.region_7.7_spmd.clone, body=%wide.region_4.6_spmd.clone.sunk | while | flops 275912704 | bytes 17376408 | solution.py:145
  73.2 2.8 fusion.107
  76.0 2.7 fusion.110
  80.2 2.8 fusion.107
  83.0 2.7 fusion.110
  87.8 2.8 fusion.107
  90.6 2.7 fusion.110
  95.4 2.8 fusion.107
  98.3 2.7 fusion.110
  103.1 2.8 fusion.107
  105.9 2.7 fusion.110
  110.7 2.8 fusion.107
  113.5 2.7 fusion.110
  118.3 2.8 fusion.107
  121.2 2.7 fusion.110
  126.0 2.8 fusion.107
  128.8 2.7 fusion.110
  133.6 2.8 fusion.107
  136.4 2.7 fusion.110
  141.2 2.8 fusion.107
  144.0 2.7 fusion.110
  148.8 2.8 fusion.107
  151.7 2.7 fusion.110
  156.5 2.8 fusion.107
  164.1 2.8 fusion.107
  171.7 2.8 fusion.107
  179.4 2.8 fusion.107
  187.0 2.8 fusion.107
  194.6 2.8 fusion.107
  202.2 2.8 fusion.107
  209.9 2.8 fusion.107
  217.5 2.8 fusion.107
  225.1 2.8 fusion.107
  232.8 2.8 fusion.107
  240.4 2.8 fusion.107
  248.0 2.8 fusion.107
  255.7 2.8 fusion.107
  263.3 2.8 fusion.107
  270.9 2.8 fusion.107
  278.5 2.8 fusion.107
  286.2 2.8 fusion.107
  293.8 2.8 fusion.107
  301.4 2.8 fusion.107
  309.1 2.8 fusion.107
  320.0 3.3 convolution_convert_fusion
  325.3 4.0 all-to-all-start
  329.2 4.1 all-to-all-done
  333.3 18.9 %reduce-scatter.2.cloned.1.call-done = bf16[128,2048]{1,0:T(8,128)(2,1)} async-done(((bf16[512,2048]{1,0:T(8,128)(2,1)}), bf16[128,2048]{1,0:T(8,128)(2,1)}) %reduce-scatter.2.cloned.1.call-update) | async-done | bytes 524304 | tf_op jit(solution)/shard_map/reduce_scatter | solution.py:165
  359.5 4.4 scatter_custom_fusion
  363.9 4.1 reshape.459
  368.0 38.8 %all_to_all.19 = bf16[128,4,2048]{2,1,0:T(4,128)(2,1)S(1)} all-to-all(bf16[128,4,2048]{2,1,0:T(4,128)(2,1)} %reshape.459), channel_id=1, replica_groups=mesh['sp'=32,'tp'=4] {'sp','tp'}, dimensions={0} | all-to-all | bytes 4194304 | tf_op jit(solution)/shard_map/all_to_all | solution.py:194
  408.2 3.4 fusion.30
  411.6 7.5 %convolution_convert_fusion.1 = bf16[128,4,2048]{2,0,1:T(8,128)(2,1)} fusion(bf16[1,512,2048]{2,1,0:T(8,128)(2,1)S(1)} %copy-done, bf16[1,2048,512]{2,1,0:T(8,128)(2,1)} %param.36, bf16[128,4,2048]{2,1,0:T(4,128)(2,1)} %copy-done.4, f32[128,1,4,512]{3,0,2,1:T(8,128)} %fusion.30), kind=kOutput, calls=%fused_computation.36 | convolution fusion | flops 2150105088 | bytes 9437184 | tf_op jit(solution)/shard_map/sekf,efd->sekd/dot_general | solution.py:210
  419.1 4.5 copy.96
  423.6 5.1 %all-to-all-start.2 = ((bf16[128,4,2048]{2,1,0:T(4,128)(2,1)}), bf16[128,4,2048]{2,1,0:T(4,128)(2,1)}, u32[]{:S(2)}, u32[]{:S(2)}) async-start(bf16[128,4,2048]{2,1,0:T(4,128)(2,1)} %copy.96), calls=%async_computation.3 | async-start | bytes 4194304 | tf_op jit(solution)/shard_map/all_to_all | solution.py:211
  428.8 30.3 %all-to-all-done.2 = bf16[128,4,2048]{2,1,0:T(4,128)(2,1)} async-done(((bf16[128,4,2048]{2,1,0:T(4,128)(2,1)}), bf16[128,4,2048]{2,1,0:T(4,128)(2,1)}, u32[]{:S(2)}, u32[]{:S(2)}) %all-to-all-start.2) | async-done | bytes 2097184 | tf_op jit(solution)/shard_map/all_to_all | solution.py:211
  459.1 4.0 reshape.464
  463.1 5.2 %gather_fusion = bf16[256,2048]{1,0:T(8,128)(2,1)} fusion(bf16[512,2048]{1,0:T(8,128)(2,1)} %reshape.464, s32[1024]{0:T(1024)S(1)} %pad_clamp_fusion), kind=kCustom, calls=%fused_computation | custom fusion | bytes 2098176 | tf_op jit(solution)/shard_map/gather | solution.py:218
  468.3 3.4 reshape.468
  471.7 4.8 multiply_reduce_fusion
  (374 shorter events, 145.6 us)
Async XLA Ops:
  6.5 405.0 %copy-start = (bf16[1,512,2048]{2,1,0:T(8,128)(2,1)S(1)}, bf16[1,512,2048]{2,1,0:T(8,128)(2,1)}, u32[]{:S(2)}) copy-start(bf16[1,512,2048]{2,1,0:T(8,128)(2,1)} %param.37) | copy-start | bytes 6291460
  6.5 2.9 copy-start.7
  6.5 3.9 copy-start.6
  6.5 4.0 copy-start.8
  6.5 60.5 %all-gather.3.cloned.1.call-start = ((), (), s32[]{:S(2)}) async-start(), calls=%async_computation.4 | async-start | bytes 8650752 | tf_op jit(solution)/shard_map/all_gather | solution.py:20
  6.6 35.9 %copy-start.15 = (f32[128]{0:T(128)S(1)}, f32[128]{0:T(128)}, u32[]{:S(2)}) copy-start(f32[128]{0:T(128)} %param.26) | copy-start | bytes 1540
  10.3 341.9 %reduce-scatter.2.cloned.1.call-start = ((), (), s32[]{:S(2)}) async-start(), calls=%async_computation.5 | async-start | bytes 2621440 | tf_op jit(solution)/shard_map/reduce_scatter | solution.py:165
  76.0 2.7 copy-start.1
  83.0 2.7 copy-start.1
  90.6 2.7 copy-start.1
  98.3 2.7 copy-start.1
  105.9 2.7 copy-start.1
  113.5 2.7 copy-start.1
  121.1 2.7 copy-start.1
  128.8 2.7 copy-start.1
  136.4 2.7 copy-start.1
  144.0 2.7 copy-start.1
  151.7 2.7 copy-start.1
  159.3 2.7 copy-start.1
  166.9 2.7 copy-start.1
  174.5 2.7 copy-start.1
  182.2 2.7 copy-start.1
  189.8 2.7 copy-start.1
  197.4 2.7 copy-start.1
  205.1 2.7 copy-start.1
  212.7 2.7 copy-start.1
  220.3 2.7 copy-start.1
  228.0 2.7 copy-start.1
  235.6 2.7 copy-start.1
  243.2 2.7 copy-start.1
  250.8 2.7 copy-start.1
  258.5 2.7 copy-start.1
  266.1 2.7 copy-start.1
  273.7 2.7 copy-start.1
  281.4 2.7 copy-start.1
  289.0 2.7 copy-start.1
  296.6 2.7 copy-start.1
  304.2 2.7 copy-start.1
  311.9 2.7 copy-start.1
  316.5 0.8 copy-start.5
  323.3 0.7 copy-start.13
  323.3 28.9 %copy-start.2 = (bf16[128,2048]{1,0:T(8,128)(2,1)S(1)}, bf16[128,2048]{1,0:T(8,128)(2,1)}, u32[]{:S(2)}) copy-start(bf16[128,2048]{1,0:T(8,128)(2,1)} %param.30) | copy-start | bytes 1572868
  324.0 31.1 %copy-start.9 = (f32[2048]{0:T(1024)S(1)}, f32[2048]{0:T(1024)}, u32[]{:S(2)}) copy-start(f32[2048]{0:T(1024)} %param.32) | copy-start | bytes 24580
  324.0 31.1 %copy-start.10 = (f32[2048]{0:T(1024)S(1)}, f32[2048]{0:T(1024)}, u32[]{:S(2)}) copy-start(f32[2048]{0:T(1024)} %param.31) | copy-start | bytes 24580
  325.3 8.0 %all-to-all-start = ((f32[4,1,128]{2,1,0:T(1,128)}), f32[4,1,128]{2,1,0:T(1,128)S(1)}, u32[]{:S(2)}, u32[]{:S(2)}) async-start(f32[4,1,128]{2,1,0:T(1,128)} %bitcast.17), calls=%async_computation.1 | async-start | bytes 4096 | tf_op jit(solution)/shard_map/all_to_all | solution.py:31
  352.2 2.9 copy-start.3
  368.0 40.1 %copy-start.16 = (bf16[1,2048,512]{2,1,0:T(8,128)(2,1)S(1)}, bf16[1,2048,512]{2,1,0:T(8,128)(2,1)}, u32[]{:S(2)}) copy-start(bf16[1,2048,512]{2,1,0:T(8,128)(2,1)} %param.35) | copy-start | bytes 6291460
  406.9 1.3 copy-start.4
  423.6 5.1 %copy-start.14 = (f32[128,2]{0,1:T(2,128)S(1)}, f32[128,2]{0,1:T(2,128)}, u32[]{:S(2)}) copy-start(f32[128,2]{0,1:T(2,128)} %param.34) | copy-start | bytes 3076
  423.6 35.5 %all-to-all-start.2 = ((bf16[128,4,2048]{2,1,0:T(4,128)(2,1)}), bf16[128,4,2048]{2,1,0:T(4,128)(2,1)}, u32[]{:S(2)}, u32[]{:S(2)}) async-start(bf16[128,4,2048]{2,1,0:T(4,128)(2,1)} %copy.96), calls=%async_computation.3 | async-start | bytes 4194304 | tf_op jit(solution)/shard_map/all_to_all | solution.py:211
  476.5 0.7 copy-start.11
  476.5 0.7 copy-start.12
Sparse Core Ops, SparseCore 0:
  10.5 56.5 all-gather.2
  323.5 28.6 reduce-scatter.1
where the time goes:
time: 488 us; the launch traced here: 485 us
  matrix products  190 us (39%)
  other arithmetic  80.6 us (17%)
  waiting for transfers between devices  77.6 us (16%)
  blocking collectives  65.9 us (14%)
  local copies, waits for them, and re-layouts  44.3 us (9%)
  between operations  16.1 us (3%)
  starting transfers between devices  9.12 us (2%)
    dot_general x32, matrix products, advance(): jnp.einsum('qkgd,tkd->kgqt', query_rot, key_block, preferred_element_type...  89.6 us
    dot_general x32, matrix products, advance(): jnp.einsum('kgqt,tkd->kgqd', weights.astype(jnp.bfloat16), value_block, p...  86.5 us
    add x32, other arithmetic, advance(): new_total = running_total * rescale + jnp.sum(weights, axis=-1)  40.1 us
    all_to_all x1, blocking collectives, per_device(): lax.all_to_all(outbound.reshape(expert_total, capacity, model_width), ('s...  38.8 us
    all_to_all x1, waiting for transfers between devices, per_device(): lax.all_to_all(served.astype(jnp.bfloat16).reshape(arrived.shape), ('sp',...  30.3 us
    all_gather x1, blocking collectives, per_device(): lax.all_gather(documents, 'sp', axis=0, tiled=True)  27.1 us
    all_gather x1, waiting for transfers between devices, sent_together(): filled = lax.all_gather(both, axis, axis=dim, tiled=True)  24.3 us
    reduce_scatter x1, waiting for transfers between devices, per_device(): lax.psum_scatter(jnp.dot(scaled, own_rows, preferred_element_type=jnp.flo...  18.9 us
  transfers between devices with their start and end apart: 4, of which 4 were waited for; matrix products, arithmetic and copies ran while one was open for 1% of the time, Pallas kernels for 0%

commit v1 on v0

v1 whole, which is shorter than its diff:
```python
import numpy as np

import jax
import jax.numpy as jnp
from jax import lax
from jax.experimental import pallas as pl
from jax.experimental.pallas import tpu as pltpu
from jax.sharding import PartitionSpec as P

HEAD = 128
GRID = 64
TP = 4
SHARE = 4
LANES = 128
TILE = 1024
APART = 32768.0
CAPACITY = 4
PARTS = 4
MARKS = 16

eps_norm = 1e-06
alpha_mix = 8.0**0.25
theta_base = 10000.0
score_scale = HEAD**-0.5 * 1.4426950408889634
f32 = jnp.float32
bf16 = jnp.bfloat16


def angle_tables(row_count):
    pair_count = HEAD // 4
    inv_freq = np.power(
        np.float32(theta_base), -np.arange(pair_count, dtype=np.float32) / np.float32(pair_count)
    ).astype(np.float32)

    def both(count):
        angles = (np.arange(count, dtype=np.float32)[:, None] * inv_freq[None, :]).astype(np.float32)
        return np.cos(angles.astype(np.float64)), np.sin(angles.astype(np.float64))

    row_cos, row_sin = both(row_count)
    col_cos, col_sin = both(GRID)
    none_row, none_col = np.zeros_like(row_cos), np.zeros_like(col_cos)
    row_c = np.concatenate([row_cos, none_row, row_cos, none_row], axis=1)
    row_s = np.concatenate([-row_sin, none_row, row_sin, none_row], axis=1)
    col_c = np.concatenate([none_col, col_cos, none_col, col_cos], axis=1)
    col_s = np.concatenate([none_col, -col_sin, none_col, col_sin], axis=1)
    return np.concatenate([row_c, row_s, col_c, col_s], axis=0).astype(np.float32)


def tables_at(table_ref, first, grid_rows):
    row_count = (table_ref.shape[0] - 2 * GRID) // 2

    def table_of(row_first, col_first):
        row_part = table_ref[pl.ds(pl.multiple_of(row_first, 8), grid_rows)]
        col_part = table_ref[col_first : col_first + GRID]
        return (row_part[:, None, :] + col_part[None, :, :]).reshape(grid_rows * GRID, HEAD)

    return (
        table_of(first, 2 * row_count),
        table_of(row_count + first, 2 * row_count + GRID),
    )


def normed_rotated(values, gain_row, cosine, sine):
    inv_rms = lax.rsqrt(jnp.mean(values * values, axis=-1, keepdims=True) + eps_norm)
    values = values * inv_rms * gain_row
    return (values * cosine + pltpu.roll(values, HEAD // 2, 1) * sine).astype(bf16)


def key_kernel(
    index_ref, key_hbm, value_hbm, doc_hbm, gain_hbm, table_hbm, out_hbm,
    key_ref, value_ref, doc_ref, gain_ref, table_ref, built_ref, in_sems, out_sems,
):
    pairs = (
        (key_hbm, key_ref), (value_hbm, value_ref), (doc_hbm, doc_ref), (gain_hbm, gain_ref),
        (table_hbm, table_ref),
    )
    arriving = [pltpu.make_async_copy(a, b, in_sems.at[i]) for i, (a, b) in enumerate(pairs)]
    for copy in arriving:
        copy.start()
    for copy in arriving:
        copy.wait()
    tok_rows = key_ref.shape[0]
    grid_rows = tok_rows // GRID
    cosine, sine = tables_at(table_ref, index_ref[0] * grid_rows, grid_rows)
    rotated = normed_rotated(key_ref[...].astype(f32), gain_ref[...], cosine, sine)
    numbers = lax.broadcasted_iota(jnp.int32, (MARKS, tok_rows), 0)
    documents = doc_ref[...]
    marks = jnp.where(numbers == documents, 1.0, 0.0)
    marks = jnp.where(numbers == MARKS - 1, documents.astype(f32), marks).astype(bf16)
    built_ref[:HEAD, :] = jnp.transpose(rotated.astype(f32)).astype(bf16)
    built_ref[HEAD : HEAD + MARKS, :] = marks
    for g in range(tok_rows // HEAD):
        built_ref[HEAD + MARKS :, g * HEAD : (g + 1) * HEAD] = value_ref[
            g * HEAD : (g + 1) * HEAD, :
        ]
    leaving = [
        pltpu.make_async_copy(built_ref, out_hbm.at[i], out_sems.at[i])
        for i in range(out_hbm.shape[0])
    ]
    for copy in leaving:
        copy.start()
    for copy in leaving:
        copy.wait()


def query_kernel(index_ref, *refs):
    query_refs = refs[:SHARE]
    gain_ref, table_ref, out_hbm, out_ref, out_sems = refs[SHARE:]
    tok_rows = query_refs[0].shape[0] - MARKS
    width = query_refs[0].shape[1]
    grid_rows = tok_rows // GRID
    own = index_ref[0] % SHARE
    numbers = lax.broadcasted_iota(jnp.int32, (LANES, tok_rows), 0).astype(f32)
    for i, query_ref in enumerate(query_refs):
        place = own ^ i
        cosine, sine = tables_at(
            table_ref, (index_ref[0] - own + place) * grid_rows, grid_rows
        )
        lines = query_ref[tok_rows:, :].astype(f32)
        documents = jnp.concatenate([lines[k : k + 1] for k in range(tok_rows // width)], axis=1)
        apart = jnp.where(numbers == documents, 0.0, -APART)
        apart = jnp.where(numbers >= MARKS - 2, 0.0, apart)
        apart = jnp.where(numbers == MARKS - 2, documents, apart)
        apart = jnp.transpose(apart).astype(bf16)
        rows = pl.ds(pl.multiple_of(place * tok_rows, tok_rows), tok_rows)
        for h in range(out_ref.shape[0]):
            values = query_ref[:tok_rows, h * HEAD : (h + 1) * HEAD].astype(f32)
            out_ref[h, rows, :HEAD] = normed_rotated(values, gain_ref[...], cosine, sine)
            out_ref[h, rows, HEAD:] = apart
    leaving = [
        pltpu.make_async_copy(out_ref.at[h], out_hbm.at[h], out_sems.at[h])
        for h in range(out_ref.shape[0])
    ]
    for copy in leaving:
        copy.start()
    for copy in leaving:
        copy.wait()


def attention_kernel(
    small_ref, query_hbm, kv_ref, out_ref, keys_ref, first_ref, last_ref, acc_ref, total_ref,
    max_ref, tiles_ref, sems,
):
    heads, _, depth = query_hbm.shape
    shards, _, tok_rows = kv_ref.shape
    rows = acc_ref.shape[0]
    tile = rows // heads
    marked = HEAD + MARKS
    step = pl.program_id(0)
    steps = query_hbm.shape[1] // tile
    arriving = [
        pltpu.make_async_copy(
            query_hbm.at[:, pl.ds(i * tile, tile), :], tiles_ref.at[i], sems.at[i]
        )
        for i in range(steps)
    ]

    @pl.when(step == 0)
    def fetch():
        for copy in arriving:
            copy.start()


    @pl.when(step == 0)
    def fill():
        for j in range(shards):
            keys_ref[j, :marked, :] = kv_ref[j, :marked, :]
            keys_ref[j, marked:, :] = jnp.zeros((depth - marked, tok_rows), bf16)
            line = kv_ref[j, HEAD:marked, :].astype(f32)
            first_ref[j] = line[MARKS - 1, 0].astype(jnp.int32)
            last_ref[j] = line[MARKS - 1, tok_rows - 1].astype(jnp.int32)

    for i in range(steps):
        pl.when(step == i)(arriving[i].wait)
    query_ref = tiles_ref.at[step]
    queries = query_ref[...].reshape(rows, depth)
    top = query_ref[0, :16, HEAD:].astype(f32)
    bottom = query_ref[0, tile - 16 :, HEAD:].astype(f32)
    low = top[0, MARKS - 2].astype(jnp.int32)
    high = bottom[15, MARKS - 2].astype(jnp.int32)
    from_shard = jnp.int32(0)
    to_shard = jnp.int32(0)
    for j in range(shards):
        from_shard += (last_ref[j] < low).astype(jnp.int32)
        to_shard += (first_ref[j] <= high).astype(jnp.int32)

    acc_ref[...] = jnp.zeros_like(acc_ref)
    total_ref[...] = jnp.zeros_like(total_ref)

    def scores_of(j):
        return jnp.dot(queries, keys_ref[j], preferred_element_type=f32)

    def values_of(j):
        return jnp.concatenate(
            [kv_ref[j, marked:, g * HEAD : (g + 1) * HEAD] for g in range(tok_rows // HEAD)],
            axis=0,
        )

    def folded(weights):
        part = weights[:, :LANES]
        for i in range(1, weights.shape[1] // LANES):
            part = part + weights[:, i * LANES : (i + 1) * LANES]
        return part

    @pl.when(small_ref[0] == 1)
    def without_max():
        max_ref[...] = jnp.zeros_like(max_ref)

        def advance(j, unused):
            weights = jnp.exp2(scores_of(j) * score_scale)
            total_ref[...] += folded(weights)
            acc_ref[...] += jnp.dot(
                weights.astype(bf16), values_of(j), preferred_element_type=f32
            )
            return unused

        lax.fori_loop(from_shard, to_shard, advance, 0)

    @pl.when(small_ref[0] == 0)
    def with_max():
        max_ref[...] = jnp.full_like(max_ref, -1e30)

        def advance(j, unused):
            scores = scores_of(j) * score_scale
            old_max = max_ref[...]
            new_max = jnp.maximum(old_max, jnp.max(scores, axis=1, keepdims=True))
            weights = jnp.exp2(scores - new_max[:, :1])
            rescale = jnp.exp2(old_max - new_max)
            max_ref[...] = new_max
            total_ref[...] = total_ref[...] * rescale + folded(weights)
            acc_ref[...] = acc_ref[...] * rescale + jnp.dot(
                weights.astype(bf16), values_of(j), preferred_element_type=f32
            )
            return unused

        lax.fori_loop(from_shard, to_shard, advance, 0)

    rows_out = LANES
    eye = lax.broadcasted_iota(jnp.int32, (rows_out, LANES), 0) == lax.broadcasted_iota(
        jnp.int32, (rows_out, LANES), 1
    )
    for h in range(heads):
        for i in range(tile // rows_out):
            mine = slice(h * tile + i * rows_out, h * tile + (i + 1) * rows_out)
            lanes = slice(h * HEAD, (h + 1) * HEAD)
            total = jnp.sum(total_ref[mine], axis=1, keepdims=True)
            some = total > 0.0
            held = jnp.where(some, total, 1.0)
            out_ref[i, :rows_out, lanes] = (acc_ref[mine] / held).astype(bf16)
            level = jnp.where(some, max_ref[mine] + jnp.log2(held), -1e30)
            flat = jnp.sum(jnp.where(eye, level, 0.0), axis=0, keepdims=True)
            top = flat.astype(bf16).astype(f32)
            rest = flat - top
            middle = rest.astype(bf16).astype(f32)
            final = rest - middle
            out_ref[i, rows_out:, lanes] = jnp.concatenate(
                [top, middle, final, jnp.zeros((13, LANES), f32)], axis=0
            ).astype(bf16)


def layer_norm(stream, gain_row, bias_row):
    center = jnp.mean(stream, axis=-1, keepdims=True)
    spread = jnp.mean(jnp.square(stream - center), axis=-1, keepdims=True)
    return (stream - center) * lax.rsqrt(spread + eps_norm) * gain_row + bias_row


def middle_kernel(
    part_ref, out_gain_ref, proj_ref, residual_ref, gain_ref, bias_ref, target_ref,
    middle_ref, outbound_ref, held_ref, sem_ref,
):
    sources, _, width = part_ref.shape
    copies = [
        pltpu.make_async_copy(
            proj_ref.at[pl.ds(t * width, width)], held_ref.at[pl.ds(t * width, width)], sem_ref.at[t]
        )
        for t in range(TP)
    ]
    for copy in copies:
        copy.start()
    rows = LANES
    heads = width // HEAD
    levels = jnp.sum(part_ref[:, rows:, :].astype(f32), axis=1)
    pieces = [levels[i * TP : (i + 1) * TP] for i in range(SHARE)]
    highest = pieces[0]
    for piece in pieces[1:]:
        highest = jnp.maximum(highest, piece)
    shares = [jnp.exp2(piece - highest) for piece in pieces]
    whole = shares[0]
    for share in shares[1:]:
        whole = whole + share
    shares = jnp.concatenate([share / whole for share in shares], axis=0)
    columns = []
    for h in range(heads):
        square = jnp.concatenate(
            [
                shares[:, h * HEAD : (h + 1) * HEAD],
                jnp.zeros((LANES - sources, LANES), f32),
            ],
            axis=0,
        )
        columns.append(jnp.transpose(square))
    attended = []
    for t in range(TP):
        for h in range(heads):
            mixed = jnp.zeros((rows, HEAD), f32)
            for i in range(SHARE):
                source = i * TP + t
                mixed = mixed + columns[h][:, source : source + 1] * part_ref[
                    source, :rows, h * HEAD : (h + 1) * HEAD
                ].astype(f32)
            attended.append(mixed.astype(bf16).astype(f32))
    attention = jnp.concatenate(attended, axis=1)
    mean_square = jnp.mean(attention * attention, axis=1, keepdims=True)
    scaled = (attention * out_gain_ref[...]).astype(bf16)
    projected = jnp.zeros((rows, held_ref.shape[1]), f32)
    for t in range(TP):
        copies[t].wait()
        lanes = slice(t * width, (t + 1) * width)
        projected = projected + jnp.dot(
            scaled[:, lanes], held_ref[lanes, :], preferred_element_type=f32
        )
    projected = projected * lax.rsqrt(mean_square + eps_norm)
    middle = layer_norm(
        alpha_mix * residual_ref[...].astype(f32) + projected, gain_ref[...], bias_ref[...]
    ).astype(bf16)
    middle_ref[...] = middle
    cut = middle.shape[1] // PARTS
    stacked = jnp.concatenate([middle[:, p * cut : (p + 1) * cut] for p in range(PARTS)], axis=0)
    out_rows = outbound_ref.shape[0]
    count = 4
    some = out_rows // count
    for c in range(count):
        row = c * some + lax.broadcasted_iota(jnp.int32, (some, PARTS * rows), 0)
        part = (row // CAPACITY) % PARTS
        slot = (row // (CAPACITY * PARTS)) * CAPACITY + row % CAPACITY
        lane = lax.broadcasted_iota(jnp.int32, (some, PARTS * rows), 1)
        code = jnp.where(part == lane // rows, slot, -1)
        chosen = (code == target_ref[0:1, :]) | (code == target_ref[1:2, :])
        outbound_ref[c * some : (c + 1) * some, :] = jnp.dot(
            jnp.where(chosen, 1.0, 0.0).astype(bf16), stacked, preferred_element_type=f32
        ).astype(bf16)


def swap_matrix(size):
    group = CAPACITY * PARTS
    tiles = size // group
    row = lax.broadcasted_iota(jnp.int32, (size, size), 0)
    col = lax.broadcasted_iota(jnp.int32, (size, size), 1)
    part = row // (tiles * CAPACITY)
    tile = (row // CAPACITY) % tiles
    inner = row % CAPACITY
    return jnp.where(col == tile * group + part * CAPACITY + inner, 1.0, 0.0).astype(bf16)


def expert_kernel(arrived_ref, gate_ref, up_ref, down_ref, served_ref, rows_ref, swap_ref):
    chunk = 256
    chunks = arrived_ref.shape[0] // chunk
    cut = arrived_ref.shape[1]
    some = chunk // PARTS
    swap_ref[...] = swap_matrix(chunk)
    for c in range(chunks):
        sorted_rows = jnp.dot(
            swap_ref[...], arrived_ref[c * chunk : (c + 1) * chunk, :], preferred_element_type=f32
        ).astype(bf16)
        for p in range(PARTS):
            rows_ref[c * some : (c + 1) * some, p * cut : (p + 1) * cut] = sorted_rows[
                p * some : (p + 1) * some
            ]
    rows = rows_ref[...]
    gate = jnp.dot(rows, gate_ref[...], preferred_element_type=f32)
    up = jnp.dot(rows, up_ref[...], preferred_element_type=f32)
    hidden = (gate / (1.0 + jnp.exp(-gate)) * up).astype(bf16)
    rows_ref[...] = jnp.dot(hidden, down_ref[...], preferred_element_type=f32).astype(bf16)
    for c in range(chunks):
        stacked = jnp.concatenate(
            [
                rows_ref[c * some : (c + 1) * some, p * cut : (p + 1) * cut]
                for p in range(PARTS)
            ],
            axis=0,
        )
        served_ref[c * chunk : (c + 1) * chunk, :] = lax.dot_general(
            swap_ref[...], stacked, (((0,), (0,)), ((), ())), preferred_element_type=f32
        ).astype(bf16)


def final_kernel(
    returned_ref, target_ref, weight_ref, middle_ref, gain_ref, bias_ref, out_ref, routed_ref
):
    rows = middle_ref.shape[0]
    all_rows, cut = returned_ref.shape
    col = lax.broadcasted_iota(jnp.int32, (rows, all_rows), 1)
    part = (col // CAPACITY) % PARTS
    slot = (col // (CAPACITY * PARTS)) * CAPACITY + col % CAPACITY
    for k in range(2):
        hit = slot == target_ref[:, k : k + 1]
        weight = weight_ref[:, k : k + 1]
        for p in range(PARTS):
            chosen = jnp.where(hit & (part == p), 1.0, 0.0).astype(bf16)
            picked = jnp.dot(chosen, returned_ref[...], preferred_element_type=f32) * weight
            lanes = slice(p * cut, (p + 1) * cut)
            routed_ref[:, lanes] = picked if k == 0 else routed_ref[:, lanes] + picked
    out_ref[...] = layer_norm(
        alpha_mix * middle_ref[...].astype(f32) + routed_ref[...], gain_ref[...], bias_ref[...]
    ).astype(bf16)


def whole_vmem():
    return pl.BlockSpec(memory_space=pltpu.VMEM)


def in_hbm():
    return pl.BlockSpec(memory_space=pltpu.HBM)


def held(array):
    return pltpu.with_memory_space_constraint(array, pltpu.HBM)


def in_smem():
    return pl.BlockSpec(memory_space=pltpu.SMEM)


def params(mib, grid=0):
    more = {"dimension_semantics": ("arbitrary",)} if grid else {}
    return pltpu.CompilerParams(vmem_limit_bytes=mib << 20, **more)


def attention_call(small, shared_rot, kv_all):
    heads, all_rows, depth = shared_rot.shape
    shards, _, tok_rows = kv_all.shape
    tile = TILE
    width = heads * HEAD
    return pl.pallas_call(
        attention_kernel,
        grid=(all_rows // tile,),
        out_shape=jax.ShapeDtypeStruct((all_rows // LANES, LANES + 16, width), bf16),
        in_specs=[
            in_smem(),
            in_hbm(),
            whole_vmem(),
        ],
        out_specs=pl.BlockSpec((tile // LANES, LANES + 16, width), lambda i: (i, 0, 0)),
        scratch_shapes=[
            pltpu.VMEM((shards, depth, tok_rows), bf16),
            pltpu.SMEM((shards,), jnp.int32),
            pltpu.SMEM((shards,), jnp.int32),
            pltpu.VMEM((heads * tile, HEAD), f32),
            pltpu.VMEM((heads * tile, HEAD), f32),
            pltpu.VMEM((heads * tile, HEAD), f32),
            pltpu.VMEM((all_rows // tile, heads, tile, depth), bf16),
            pltpu.SemaphoreType.DMA((all_rows // tile,)),
        ],
        compiler_params=params(40, 1),
        name="document_attention",
    )(small, held(shared_rot), kv_all)


def per_device(
    queries, key_heads, value_heads, documents, query_gain, key_gain, out_gain, out_proj,
    residual, mid_gain, mid_bias, routes, route_weights, expert_gate, expert_up, expert_down,
    final_gain, final_bias,
):
    tok_rows, width = queries.shape
    heads = width // HEAD
    sp_size = lax.axis_size("sp")
    tp_size = lax.axis_size("tp")
    shards = sp_size // SHARE
    table = jnp.asarray(angle_tables(sp_size * tok_rows // GRID))
    index = lax.axis_index("sp").astype(jnp.int32).reshape(1)
    class_groups = [[c + SHARE * j for j in range(shards)] for c in range(SHARE)]
    owner_groups = [
        [(g * SHARE + i) * tp_size + t for i in range(SHARE) for t in range(tp_size)]
        for g in range(shards)
    ]

    kv_rows = 2 * HEAD + MARKS
    kv = pl.pallas_call(
        key_kernel,
        out_shape=pltpu.HBM((shards, kv_rows, tok_rows), bf16),
        in_specs=[in_smem()] + [in_hbm()] * 5,
        out_specs=in_hbm(),
        scratch_shapes=[
            pltpu.VMEM(key_heads.shape, bf16),
            pltpu.VMEM(value_heads.shape, bf16),
            pltpu.VMEM((1, tok_rows), jnp.int32),
            pltpu.VMEM((1, HEAD), f32),
            pltpu.VMEM(table.shape, f32),
            pltpu.VMEM((kv_rows, tok_rows), bf16),
            pltpu.SemaphoreType.DMA((5,)),
            pltpu.SemaphoreType.DMA((shards,)),
        ],
        compiler_params=params(16),
        name="key_rotation",
    )(
        index, held(key_heads), held(value_heads), held(documents.reshape(1, tok_rows)),
        held(key_gain.reshape(1, HEAD)), held(table),
    )
    kv_all = lax.all_to_all(kv, "sp", 0, 0, tiled=True, axis_index_groups=class_groups)

    lines = documents.astype(bf16).reshape(tok_rows // width, width)
    marked = jnp.concatenate(
        [queries, lines, jnp.zeros((MARKS - tok_rows // width, width), bf16)], axis=0
    )
    shared = [marked]
    for k in range(1, SHARE):
        shared.append(lax.ppermute(marked, "sp", [(i, i ^ k) for i in range(sp_size)]))

    shared_rot = pl.pallas_call(
        query_kernel,
        out_shape=pltpu.HBM((heads, SHARE * tok_rows, 2 * HEAD), bf16),
        in_specs=[in_smem()] + [whole_vmem()] * (SHARE + 2),
        out_specs=in_hbm(),
        scratch_shapes=[
            pltpu.VMEM((heads, SHARE * tok_rows, 2 * HEAD), bf16),
            pltpu.SemaphoreType.DMA((heads,)),
        ],
        compiler_params=params(24),
        name="query_rotation",
    )(index, *shared, query_gain.reshape(1, HEAD), table)

    largest = jnp.max(jnp.abs(query_gain)) * jnp.max(jnp.abs(key_gain))
    small = (largest * (HEAD * score_scale * 1.02) < 50.0).astype(jnp.int32).reshape(1)
    partial = attention_call(small, shared_rot, kv_all)
    partial = lax.all_to_all(
        partial, ("sp", "tp"), 0, 0, tiled=True, axis_index_groups=owner_groups
    )

    out_rows, model_width = residual.shape
    expert_total = sp_size * tp_size
    flat = routes.T.reshape(-1)
    order = jnp.arange(flat.shape[0], dtype=jnp.int32)
    earlier = (flat[:, None] == flat[None, :]) & (order[None, :] < order[:, None])
    rank = jnp.sum(earlier.astype(jnp.int32), axis=1)
    target = (flat * CAPACITY + rank).reshape(2, out_rows)

    cut = model_width // PARTS
    exchange_rows = expert_total * CAPACITY * PARTS
    middle, outbound = pl.pallas_call(
        middle_kernel,
        out_shape=(
            jax.ShapeDtypeStruct((out_rows, model_width), bf16),
            jax.ShapeDtypeStruct((exchange_rows, cut), bf16),
        ),
        in_specs=[
            whole_vmem(), whole_vmem(), in_hbm(), whole_vmem(),
            whole_vmem(), whole_vmem(), whole_vmem(),
        ],
        out_specs=(whole_vmem(), whole_vmem()),
        scratch_shapes=[
            pltpu.VMEM(out_proj.shape, bf16),
            pltpu.SemaphoreType.DMA((TP,)),
        ],
        compiler_params=params(40),
        name="middle_stream",
    )(
        partial, out_gain.reshape(1, -1), held(out_proj), residual, mid_gain.reshape(1, -1),
        mid_bias.reshape(1, -1), jnp.tile(target, (1, PARTS)),
    )
    arrived = lax.all_to_all(
        outbound.reshape(expert_total, CAPACITY * PARTS, cut), ("sp", "tp"), 0, 0, tiled=True
    )
    hidden_width = expert_gate.shape[2]
    served = pl.pallas_call(
        expert_kernel,
        out_shape=jax.ShapeDtypeStruct((exchange_rows, cut), bf16),
        in_specs=[whole_vmem() for _ in range(4)],
        out_specs=whole_vmem(),
        scratch_shapes=[
            pltpu.VMEM((expert_total * CAPACITY, model_width), bf16),
            pltpu.VMEM((256, 256), bf16),
        ],
        compiler_params=params(40),
        name="expert",
    )(
        arrived.reshape(exchange_rows, cut),
        expert_gate.reshape(model_width, hidden_width),
        expert_up.reshape(model_width, hidden_width),
        expert_down.reshape(hidden_width, model_width),
    )
    returned = lax.all_to_all(
        served.reshape(expert_total, CAPACITY * PARTS, cut), ("sp", "tp"), 0, 0, tiled=True
    )
    return pl.pallas_call(
        final_kernel,
        out_shape=jax.ShapeDtypeStruct((out_rows, model_width), bf16),
        in_specs=[whole_vmem() for _ in range(6)],
        out_specs=whole_vmem(),
        scratch_shapes=[pltpu.VMEM((out_rows, model_width), f32)],
        compiler_params=params(40),
        name="final_stream",
    )(
        returned.reshape(exchange_rows, cut), target.T, route_weights, middle,
        final_gain.reshape(1, -1), final_bias.reshape(1, -1),
    )


def solution(mesh):
    rows = P(("sp", "tp"), None)
    experts = P(("sp", "tp"), None, None)
    return jax.shard_map(
        per_device,
        mesh=mesh,
        in_specs=(
            P("sp", "tp"), P("sp", "tp"), P("sp", "tp"), P("sp"), P(), P(), P(), P(), rows, P(),
            P(), rows, rows, experts, experts, experts, P(), P(),
        ),
        out_specs=rows,
        check_vma=False,
    )
```

time: 488 us -> 195 us (0.40)
  matrix products: 190 us -> 0 us
  other arithmetic: 80.6 us -> 1.58 us
  Pallas kernels: 0 us -> 50.6 us
  local copies, waits for them, and re-layouts: 44.3 us -> 0.66 us
  blocking collectives: 65.9 us -> 36.8 us
  starting transfers between devices: 9.12 us -> 24.4 us
  between operations: 16.1 us -> 1.52 us
    dot_general x67 -> x0, matrix products: 190 us -> none  [the longest x32 89.6 us: advance(): jnp.einsum('qkgd,tkd->kgqt', query_rot, key_block, preferred_element_type...]
    pallas_call x0 -> x6, Pallas kernels: none -> 50.6 us  [the longest x1 29.1 us: attention_call(): pl.pallas_call(attention_kernel, grid=(all_rows // tile,), out_shape=jax....]
    add x32 -> x1, other arithmetic: 40.1 us -> 0.01 us  [per_device(): target = (flat * CAPACITY + rank).reshape(2, out_rows)]
    ppermute x0 -> x3, waiting for transfers between devices: none -> 31.8 us  [per_device(): lax.ppermute(marked, 'sp', [(i, i ^ k) for i in range(sp_size)])]
    reduce_sum x42 -> x1, other arithmetic: 28.3 us -> 0.2 us  [per_device(): rank = jnp.sum(earlier.astype(jnp.int32), axis=1)]
    all_gather x1 -> x0, blocking collectives: 27.1 us -> none  [per_device(): lax.all_gather(documents, 'sp', axis=0, tiled=True)]
    all_gather x1 -> x0, waiting for transfers between devices: 24.3 us -> none  [sent_together(): filled = lax.all_gather(both, axis, axis=dim, tiled=True)]
    reduce_scatter x1 -> x0, waiting for transfers between devices: 18.9 us -> none  [per_device(): lax.psum_scatter(jnp.dot(scaled, own_rows, preferred_element_type=jnp.flo...]
  transfers between devices with their start and end apart: 4 -> 6, of which waited for: 4 -> 4; matrix products, arithmetic and copies ran while one was open for 1% -> 1% of each run, Pallas kernels for 0% -> 2%
where the time goes in v1:
time: 195 us; the launch traced here: 194 us
  waiting for transfers between devices  78.9 us (40%)
  Pallas kernels  50.6 us (26%)
  blocking collectives  36.8 us (19%)
  starting transfers between devices  24.4 us (13%)
    all_to_all x1, blocking collectives, per_device(): lax.all_to_all(outbound.reshape(expert_total, CAPACITY * PARTS, cut), ('s...  36.8 us
    ppermute x3, waiting for transfers between devices, per_device(): lax.ppermute(marked, 'sp', [(i, i ^ k) for i in range(sp_size)])  31.8 us
    all_to_all x1, waiting for transfers between devices, per_device(): lax.all_to_all(served.reshape(expert_total, CAPACITY * PARTS, cut), ('sp'...  30.8 us
    pallas_call x1, Pallas kernels, attention_call(): pl.pallas_call(attention_kernel, grid=(all_rows // tile,), out_shape=jax....  29.1 us
    all_to_all x1, waiting for transfers between devices, per_device(): lax.all_to_all(partial, ('sp', 'tp'), 0, 0, tiled=True, axis_index_groups...  16.4 us
    all_to_all x1, starting transfers between devices, per_device(): lax.all_to_all(partial, ('sp', 'tp'), 0, 0, tiled=True, axis_index_groups...  9.05 us
    all_to_all x1, starting transfers between devices, per_device(): lax.all_to_all(kv, 'sp', 0, 0, tiled=True, axis_index_groups=class_groups)  8.63 us
    pallas_call x1, Pallas kernels, per_device(): pl.pallas_call(expert_kernel, out_shape=jax.ShapeDtypeStruct((exchange_ro...  5.93 us
  transfers between devices with their start and end apart: 6, of which 4 were waited for; matrix products, arithmetic and copies ran while one was open for 1% of the time, Pallas kernels for 2%

profile of v1, /device:TPU:1, one launch (start us, length us, event | category | flops | bytes accessed | tf_op | source)
XLA Modules:
  0.0 194.5 jit_solution(24648565162786878)
XLA Ops:
  0.0 2.9 %key_rotation.1 = bf16[8,272,512]{2,1,0:T(8,128)(2,1)} custom-call(s32[1]{0:T(128)} %bitcast.1.index_ref, bf16[512,128]{1,0:T(8,128)(2,1)} %key_hbm.1, bf16[512,128]{1,0:T(8,128)(2,1)} %value_hbm.1, s32[1,512]{1,0:T(1,128)} %bitcast.43, f32[1,128]{1,0:T(1,128)} %bitcast.45, f32[640,128]{1,0:T(8,128)} %constant.20.clone.refs_5_.table_hbm), custom_call_target="tpu_custom_call" | custom-call | tf_op jit(solution)/shard_map/key_rotation/pallas_call | solution.py:478
  2.9 0.0 copy-start.12
  3.0 0.0 copy-start.11
  3.0 0.0 copy-start.15
  3.0 0.0 copy-start.10
  3.0 0.0 copy-start.3
  3.0 8.6 %all-to-all-start = ((bf16[8,272,512]{2,1,0:T(8,128)(2,1)}), bf16[8,272,512]{2,1,0:T(8,128)(2,1)S(1)}, u32[]{:S(2)}, u32[]{:S(2)}) async-start(bf16[8,272,512]{2,1,0:T(8,128)(2,1)} %key_rotation.1), calls=%async_computation | async-start | bytes 4456448 | tf_op jit(solution)/shard_map/all_to_all | solution.py:499
  11.6 0.0 copy-done.12
  11.7 0.1 pad.2.clone
  11.7 0.0 copy-done.11
  11.8 0.1 maximum_maximum_fusion.refs_0_
  11.9 1.0 collective-permute-start
  12.9 0.4 collective-permute-start.1
  13.3 1.3 collective-permute-start.2
  14.7 0.0 copy-done.15
  14.7 0.6 abs_reduce_fusion
  15.3 0.0 copy-done.10
  15.3 0.6 abs_reduce_fusion.1
  17.2 0.0 collective-permute-done.refs_1_
  17.2 25.0 %collective-permute-done.1.refs_2_ = bf16[528,256]{1,0:T(8,128)(2,1)S(1)} collective-permute-done((bf16[528,256]{1,0:T(8,128)(2,1)S(1)}, bf16[528,256]{1,0:T(8,128)(2,1)S(1)}, u32[]{:S(2)}, u32[]{:S(2)}) %collective-permute-start.1) | collective-permute-done | bytes 270368 | tf_op jit(solution)/shard_map/ppermute | solution.py:507
  42.2 6.7 %collective-permute-done.2.refs_3_ = bf16[528,256]{1,0:T(8,128)(2,1)} collective-permute-done((bf16[528,256]{1,0:T(8,128)(2,1)S(1)}, bf16[528,256]{1,0:T(8,128)(2,1)}, u32[]{:S(2)}, u32[]{:S(2)}) %collective-permute-start.2) | collective-permute-done | bytes 270368 | tf_op jit(solution)/shard_map/ppermute | solution.py:507
  49.0 0.0 copy-done.3
  49.0 4.0 %query_rotation.1.query_hbm = bf16[2,2048,256]{2,1,0:T(8,128)(2,1)} custom-call(s32[1]{0:T(128)} %bitcast.1.index_ref, bf16[528,256]{1,0:T(8,128)(2,1)S(1)} %maximum_maximum_fusion.refs_0_, bf16[528,256]{1,0:T(8,128)(2,1)S(1)} %collective-permute-done.refs_1_, bf16[528,256]{1,0:T(8,128)(2,1)S(1)} %collective-permute-done.1.refs_2_, ...), custom_call_target="tpu_custom_call" | custom-call | tf_op jit(solution)/shard_map/query_rotation/pallas_call | solution.py:509
  53.0 0.0 all-to-all-done.kv_ref
  53.0 29.1 %document_attention.1 = bf16[16,144,256]{2,1,0:T(8,128)(2,1)} custom-call(s32[1]{0:T(128)} %bitcast.small_ref, bf16[2,2048,256]{2,1,0:T(8,128)(2,1)} %query_rotation.1.query_hbm, bf16[8,272,512]{2,1,0:T(8,128)(2,1)S(1)} %all-to-all-done.kv_ref), custom_call_target="tpu_custom_call" | custom-call | tf_op jit(solution)/shard_map/document_attention/pallas_call | solution.py:434
  82.1 0.0 copy-start.13
  82.1 0.0 copy-start.4
  82.2 0.0 copy-start.5
  82.2 0.0 copy-start.6
  82.2 0.0 copy-start.9
  82.2 9.0 %all-to-all-start.1 = ((bf16[16,144,256]{2,1,0:T(8,128)(2,1)}), bf16[16,144,256]{2,1,0:T(8,128)(2,1)S(1)}, u32[]{:S(2)}, u32[]{:S(2)}) async-start(bf16[16,144,256]{2,1,0:T(8,128)(2,1)} %document_attention.1), calls=%async_computation.1 | async-start | bytes 2359296 | tf_op jit(solution)/shard_map/all_to_all | solution.py:525
  91.2 0.0 copy-done.13
  91.2 0.1 copy.33
  91.4 0.1 copy.35
  91.4 0.2 convert_reduce_fusion
  91.6 0.1 copy.36
  91.8 0.1 copy.37
  91.8 16.4 %all-to-all-done.1.part_ref = bf16[16,144,256]{2,1,0:T(8,128)(2,1)S(1)} async-done(((bf16[16,144,256]{2,1,0:T(8,128)(2,1)}), bf16[16,144,256]{2,1,0:T(8,128)(2,1)S(1)}, u32[]{:S(2)}, u32[]{:S(2)}) %all-to-all-start.1) | async-done | bytes 1179680 | tf_op jit(solution)/shard_map/all_to_all | solution.py:525
  108.2 0.0 copy-done.4
  108.2 0.0 copy-done.5
  108.2 0.0 copy-done.6
  108.2 0.0 copy-done.9
  108.2 0.0 copy-start.2
  108.3 5.1 %middle_stream.1 = (bf16[128,2048]{1,0:T(8,128)(2,1)S(1)}, bf16[2048,512]{1,0:T(8,128)(2,1)S(1)}) custom-call(bf16[16,144,256]{2,1,0:T(8,128)(2,1)S(1)} %all-to-all-done.1.part_ref, f32[1,1024]{1,0:T(1,128)S(1)} %bitcast.39, bf16[1024,2048]{1,0:T(8,128)(2,1)} %proj_ref.1, bf16[128,2048]{1,0:T(8,128)(2,1)S(1)} %copy-done.4, f32[1,2048]{1,0:T(1,128)S(1)} %bitcast.35, ...), custom_call_target="tpu_custom_call" | custom-call | tf_op jit(solution)/shard_map/middle_stream/pallas_call | solution.py:539
  113.3 0.0 copy-start
  113.4 0.0 copy-start.1
  113.4 36.8 %all_to_all.20 = bf16[128,16,512]{2,1,0:T(8,128)(2,1)S(1)} all-to-all(bf16[128,16,512]{2,1,0:T(8,128)(2,1)S(1)} %bitcast.32), channel_id=1, replica_groups=mesh['sp'=32,'tp'=4] {'sp','tp'}, dimensions={0} | all-to-all | bytes 4194304 | tf_op jit(solution)/shard_map/all_to_all | solution.py:560
  150.2 0.0 copy-done.2
  150.2 0.0 copy-done
  150.2 0.0 copy-done.1
  150.2 5.9 %expert.1 = bf16[2048,512]{1,0:T(8,128)(2,1)} custom-call(bf16[2048,512]{1,0:T(8,128)(2,1)S(1)} %bitcast.27, bf16[2048,512]{1,0:T(8,128)(2,1)S(1)} %bitcast.29, bf16[2048,512]{1,0:T(8,128)(2,1)S(1)} %bitcast.30, bf16[512,2048]{1,0:T(8,128)(2,1)S(1)} %bitcast.31), custom_call_target="tpu_custom_call" | custom-call | tf_op jit(solution)/shard_map/expert/pallas_call | solution.py:564
  156.1 0.0 copy-start.14
  156.1 0.0 copy-start.7
  156.1 0.0 copy-start.8
  156.1 3.9 %all-to-all-start.3 = ((bf16[128,16,512]{2,1,0:T(8,128)(2,1)}), bf16[128,16,512]{2,1,0:T(8,128)(2,1)S(1)}, u32[]{:S(2)}, u32[]{:S(2)}) async-start(bf16[128,16,512]{2,1,0:T(8,128)(2,1)} %bitcast.16), calls=%async_computation.3 | async-start | bytes 4194304 | tf_op jit(solution)/shard_map/all_to_all | solution.py:581
  160.0 0.0 copy-done.14
  160.1 0.1 copy.38.weight_ref
  160.2 30.8 %all-to-all-done.3 = bf16[128,16,512]{2,1,0:T(8,128)(2,1)S(1)} async-done(((bf16[128,16,512]{2,1,0:T(8,128)(2,1)}), bf16[128,16,512]{2,1,0:T(8,128)(2,1)S(1)}, u32[]{:S(2)}, u32[]{:S(2)}) %all-to-all-start.3) | async-done | bytes 2097184 | tf_op jit(solution)/shard_map/all_to_all | solution.py:581
  190.9 0.0 copy-done.7
  190.9 0.0 copy-done.8
  191.0 3.5 %final_stream.1 = bf16[128,2048]{1,0:T(8,128)(2,1)} custom-call(bf16[2048,512]{1,0:T(8,128)(2,1)S(1)} %bitcast.28, s32[128,2]{1,0:T(8,128)S(1)} %bitcast.33, f32[128,2]{1,0:T(8,128)S(1)} %copy.38.weight_ref, bf16[128,2048]{1,0:T(8,128)(2,1)S(1)} %get-tuple-element.8.middle_ref, f32[1,2048]{1,0:T(1,128)S(1)} %bitcast.37, f32[1,2048]{1,0:T(1,128)S(1)} %bitcast.38), custom_call_target="tpu_custom_call" | custom-call | tf_op jit(solution)/shard_map/final_stream/pallas_call | solution.py:584
  (6 shorter events, 0.0 us)
Async XLA Ops:
  2.9 8.7 %copy-start.12 = (s32[512]{0:T(512)S(1)}, s32[512]{0:T(512)}, u32[]{:S(2)}) copy-start(s32[512]{0:T(512)} %param.22) | copy-start | bytes 6148
  3.0 8.8 %copy-start.11 = (bf16[512,256]{1,0:T(8,128)(2,1)S(1)}, bf16[512,256]{1,0:T(8,128)(2,1)}, u32[]{:S(2)}) copy-start(bf16[512,256]{1,0:T(8,128)(2,1)} %param.19) | copy-start | bytes 786436
  3.0 11.7 %copy-start.15 = (f32[128]{0:T(128)S(1)}, f32[128]{0:T(128)}, u32[]{:S(2)}) copy-start(f32[128]{0:T(128)} %param.24) | copy-start | bytes 1540
  3.0 12.3 %copy-start.10 = (f32[128]{0:T(128)S(1)}, f32[128]{0:T(128)}, u32[]{:S(2)}) copy-start(f32[128]{0:T(128)} %param.23) | copy-start | bytes 1540
  3.0 46.0 %copy-start.3 = (f32[640,128]{1,0:T(8,128)S(1)}, f32[640,128]{1,0:T(8,128)}, u32[]{:S(2)}) copy-start(f32[640,128]{1,0:T(8,128)} %constant.20.clone.refs_5_.table_hbm) | copy-start | bytes 983044
  3.0 50.0 %all-to-all-start = ((bf16[8,272,512]{2,1,0:T(8,128)(2,1)}), bf16[8,272,512]{2,1,0:T(8,128)(2,1)S(1)}, u32[]{:S(2)}, u32[]{:S(2)}) async-start(bf16[8,272,512]{2,1,0:T(8,128)(2,1)} %key_rotation.1), calls=%async_computation | async-start | bytes 4456448 | tf_op jit(solution)/shard_map/all_to_all | solution.py:499
  11.9 5.3 %collective-permute-start = (bf16[528,256]{1,0:T(8,128)(2,1)S(1)}, bf16[528,256]{1,0:T(8,128)(2,1)S(1)}, u32[]{:S(2)}, u32[]{:S(2)}) collective-permute-start(bf16[528,256]{1,0:T(8,128)(2,1)S(1)} %maximum_maximum_fusion.refs_0_), channel_id=1, source_target_pairs={{0,4},{4,0},{8,12},{12,8},{16,20},{20,16},{24,28},{28,24},{32,36},... | collective-permute-start | bytes 811016 | tf_op jit(solution)/shard_map/ppermute | solution.py:507
  12.9 29.3 %collective-permute-start.1 = (bf16[528,256]{1,0:T(8,128)(2,1)S(1)}, bf16[528,256]{1,0:T(8,128)(2,1)S(1)}, u32[]{:S(2)}, u32[]{:S(2)}) collective-permute-start(bf16[528,256]{1,0:T(8,128)(2,1)S(1)} %maximum_maximum_fusion.refs_0_), channel_id=1, source_target_pairs={{0,8},{4,12},{8,0},{12,4},{16,24},{20,28},{24,16},{28,20},{32,40},... | collective-permute-start | bytes 811016 | tf_op jit(solution)/shard_map/ppermute | solution.py:507
  13.3 35.6 %collective-permute-start.2 = (bf16[528,256]{1,0:T(8,128)(2,1)S(1)}, bf16[528,256]{1,0:T(8,128)(2,1)}, u32[]{:S(2)}, u32[]{:S(2)}) collective-permute-start(bf16[528,256]{1,0:T(8,128)(2,1)S(1)} %maximum_maximum_fusion.refs_0_), channel_id=1, source_target_pairs={{0,12},{4,8},{8,4},{12,0},{16,28},{20,24},{24,20},{28,16},{32,44},... | collective-permute-start | bytes 811016 | tf_op jit(solution)/shard_map/ppermute | solution.py:507
  82.1 9.1 %copy-start.13 = (s32[128,2]{0,1:T(2,128)S(1)}, s32[128,2]{0,1:T(2,128)}, u32[]{:S(2)}) copy-start(s32[128,2]{0,1:T(2,128)} %param.30) | copy-start | bytes 3076
  82.1 26.1 %copy-start.4 = (bf16[128,2048]{1,0:T(8,128)(2,1)S(1)}, bf16[128,2048]{1,0:T(8,128)(2,1)}, u32[]{:S(2)}) copy-start(bf16[128,2048]{1,0:T(8,128)(2,1)} %residual_ref.1) | copy-start | bytes 1572868
  82.2 26.1 %copy-start.5 = (f32[2048]{0:T(1024)S(1)}, f32[2048]{0:T(1024)}, u32[]{:S(2)}) copy-start(f32[2048]{0:T(1024)} %param.28) | copy-start | bytes 24580
  82.2 26.1 %copy-start.6 = (f32[2048]{0:T(1024)S(1)}, f32[2048]{0:T(1024)}, u32[]{:S(2)}) copy-start(f32[2048]{0:T(1024)} %param.29) | copy-start | bytes 24580
  82.2 26.1 %copy-start.9 = (f32[1024]{0:T(1024)S(1)}, f32[1024]{0:T(1024)}, u32[]{:S(2)}) copy-start(f32[1024]{0:T(1024)} %param.25) | copy-start | bytes 12292
  82.2 26.0 %all-to-all-start.1 = ((bf16[16,144,256]{2,1,0:T(8,128)(2,1)}), bf16[16,144,256]{2,1,0:T(8,128)(2,1)S(1)}, u32[]{:S(2)}, u32[]{:S(2)}) async-start(bf16[16,144,256]{2,1,0:T(8,128)(2,1)} %document_attention.1), calls=%async_computation.1 | async-start | bytes 2359296 | tf_op jit(solution)/shard_map/all_to_all | solution.py:525
  108.2 41.9 %copy-start.2 = (bf16[1,512,2048]{2,1,0:T(8,128)(2,1)S(1)}, bf16[1,512,2048]{2,1,0:T(8,128)(2,1)}, u32[]{:S(2)}) copy-start(bf16[1,512,2048]{2,1,0:T(8,128)(2,1)} %param.34) | copy-start | bytes 6291460
  113.3 36.8 %copy-start = (bf16[1,2048,512]{2,1,0:T(8,128)(2,1)S(1)}, bf16[1,2048,512]{2,1,0:T(8,128)(2,1)}, u32[]{:S(2)}) copy-start(bf16[1,2048,512]{2,1,0:T(8,128)(2,1)} %param.32) | copy-start | bytes 6291460
  113.4 36.8 %copy-start.1 = (bf16[1,2048,512]{2,1,0:T(8,128)(2,1)S(1)}, bf16[1,2048,512]{2,1,0:T(8,128)(2,1)}, u32[]{:S(2)}) copy-start(bf16[1,2048,512]{2,1,0:T(8,128)(2,1)} %param.33) | copy-start | bytes 6291460
  156.1 3.9 %copy-start.14 = (f32[128,2]{0,1:T(2,128)S(1)}, f32[128,2]{0,1:T(2,128)}, u32[]{:S(2)}) copy-start(f32[128,2]{0,1:T(2,128)} %param.31) | copy-start | bytes 3076
  156.1 34.8 %copy-start.7 = (f32[2048]{0:T(1024)S(1)}, f32[2048]{0:T(1024)}, u32[]{:S(2)}) copy-start(f32[2048]{0:T(1024)} %param.35) | copy-start | bytes 24580
  156.1 34.8 %copy-start.8 = (f32[2048]{0:T(1024)S(1)}, f32[2048]{0:T(1024)}, u32[]{:S(2)}) copy-start(f32[2048]{0:T(1024)} %param.36) | copy-start | bytes 24580
  156.1 34.8 %all-to-all-start.3 = ((bf16[128,16,512]{2,1,0:T(8,128)(2,1)}), bf16[128,16,512]{2,1,0:T(8,128)(2,1)S(1)}, u32[]{:S(2)}, u32[]{:S(2)}) async-start(bf16[128,16,512]{2,1,0:T(8,128)(2,1)} %bitcast.16), calls=%async_computation.3 | async-start | bytes 4194304 | tf_op jit(solution)/shard_map/all_to_all | solution.py:581

commit v2 on v1

--- a/solution.py
+++ b/solution.py
@@ -12,10 +12,11 @@
 TP = 4
 SHARE = 4
 LANES = 128
-TILE = 1024
+TILE = 2048
 APART = 32768.0
 CAPACITY = 4
 PARTS = 4
+SHARDS = 8
 MARKS = 16
 
 eps_norm = 1e-06
@@ -67,9 +68,11 @@
 
 
 def key_kernel(
-    index_ref, key_hbm, value_hbm, doc_hbm, gain_hbm, table_hbm, out_hbm,
-    key_ref, value_ref, doc_ref, gain_ref, table_ref, built_ref, in_sems, out_sems,
+    index_ref, key_hbm, value_hbm, doc_hbm, gain_hbm, table_hbm, query_hbm, out_hbm, marked_hbm,
+    key_ref, value_ref, doc_ref, gain_ref, table_ref, built_ref, lines_ref, in_sems, out_sems,
 ):
+    tok_rows, width = query_hbm.shape
+    passing = pltpu.make_async_copy(query_hbm, lines_ref.at[pl.ds(0, tok_rows)], in_sems.at[5])
     pairs = (
         (key_hbm, key_ref), (value_hbm, value_ref), (doc_hbm, doc_ref), (gain_hbm, gain_ref),
         (table_hbm, table_ref),
@@ -77,9 +80,9 @@
     arriving = [pltpu.make_async_copy(a, b, in_sems.at[i]) for i, (a, b) in enumerate(pairs)]
     for copy in arriving:
         copy.start()
+    passing.start()
     for copy in arriving:
         copy.wait()
-    tok_rows = key_ref.shape[0]
     grid_rows = tok_rows // GRID
     cosine, sine = tables_at(table_ref, index_ref[0] * grid_rows, grid_rows)
     rotated = normed_rotated(key_ref[...].astype(f32), gain_ref[...], cosine, sine)
@@ -93,25 +96,43 @@
         built_ref[HEAD + MARKS :, g * HEAD : (g + 1) * HEAD] = value_ref[
             g * HEAD : (g + 1) * HEAD, :
         ]
-    leaving = [
-        pltpu.make_async_copy(built_ref, out_hbm.at[i], out_sems.at[i])
-        for i in range(out_hbm.shape[0])
+    leaving = pltpu.make_async_copy(built_ref, out_hbm, out_sems.at[0])
+    leaving.start()
+    lines = [
+        documents[:, i * width : (i + 1) * width].astype(f32) for i in range(tok_rows // width)
     ]
-    for copy in leaving:
+    lines.append(jnp.zeros((MARKS - len(lines), width), f32))
+    lines_ref[tok_rows:, :] = jnp.concatenate(lines, axis=0).astype(bf16)
+    passing.wait()
+    marking = pltpu.make_async_copy(lines_ref, marked_hbm, out_sems.at[1])
+    marking.start()
+    leaving.wait()
+    marking.wait()
+
+
+def query_kernel(index_ref, *refs):
+    query_hbms = refs[:SHARE]
+    (
+        gain_hbm, table_hbm, out_hbm, out_ref, gain_ref, table_ref, query_refs, out_sems, in_sems,
+    ) = refs[SHARE:]
+    arriving = [
+        pltpu.make_async_copy(query_hbm, query_refs.at[i], in_sems.at[2 + i])
+        for i, query_hbm in enumerate(query_hbms)
+    ] + [
+        pltpu.make_async_copy(gain_hbm, gain_ref, in_sems.at[0]),
+        pltpu.make_async_copy(table_hbm, table_ref, in_sems.at[1]),
+    ]
+    for copy in arriving:
         copy.start()
-    for copy in leaving:
+    for copy in arriving:
         copy.wait()
-
-
-def query_kernel(index_ref, *refs):
-    query_refs = refs[:SHARE]
-    gain_ref, table_ref, out_hbm, out_ref, out_sems = refs[SHARE:]
-    tok_rows = query_refs[0].shape[0] - MARKS
-    width = query_refs[0].shape[1]
+    tok_rows = query_refs.shape[1] - MARKS
+    width = query_refs.shape[2]
     grid_rows = tok_rows // GRID
     own = index_ref[0] % SHARE
     numbers = lax.broadcasted_iota(jnp.int32, (LANES, tok_rows), 0).astype(f32)
-    for i, query_ref in enumerate(query_refs):
+    for i in range(SHARE):
+        query_ref = query_refs.at[i]
         place = own ^ i
         cosine, sine = tables_at(
             table_ref, (index_ref[0] - own + place) * grid_rows, grid_rows
@@ -122,7 +143,8 @@
         apart = jnp.where(numbers >= MARKS - 2, 0.0, apart)
         apart = jnp.where(numbers == MARKS - 2, documents, apart)
         apart = jnp.transpose(apart).astype(bf16)
-        rows = pl.ds(pl.multiple_of(place * tok_rows, tok_rows), tok_rows)
+        half = 0 if i % 2 else SHARE // 2
+        rows = pl.ds(pl.multiple_of((half + place // 2) * tok_rows, tok_rows), tok_rows)
         for h in range(out_ref.shape[0]):
             values = query_ref[:tok_rows, h * HEAD : (h + 1) * HEAD].astype(f32)
             out_ref[h, rows, :HEAD] = normed_rotated(values, gain_ref[...], cosine, sine)
@@ -137,64 +159,82 @@
         copy.wait()
 
 
-def attention_kernel(
-    small_ref, query_hbm, kv_ref, out_ref, keys_ref, first_ref, last_ref, acc_ref, total_ref,
-    max_ref, tiles_ref, sems,
-):
-    heads, _, depth = query_hbm.shape
-    shards, _, tok_rows = kv_ref.shape
+def attention_kernel(query_gain_ref, key_gain_ref, query_hbm, *refs):
+    kv_refs = refs[:SHARDS]
+    refs = refs[SHARDS:]
+    (
+        out_ref, keys_ref, values_ref, first_ref, last_ref, order_ref, small_ref, acc_ref, total_ref, max_ref,
+        tiles_ref, tile_sems, key_sems, value_sems,
+    ) = refs
+    heads, all_rows, depth = query_hbm.shape
+    tok_rows = keys_ref.shape[2]
     rows = acc_ref.shape[0]
     tile = rows // heads
     marked = HEAD + MARKS
+    groups = tok_rows // HEAD
     step = pl.program_id(0)
-    steps = query_hbm.shape[1] // tile
-    arriving = [
+    steps = all_rows // tile
+    tiles = [
         pltpu.make_async_copy(
-            query_hbm.at[:, pl.ds(i * tile, tile), :], tiles_ref.at[i], sems.at[i]
+            query_hbm.at[:, pl.ds(i * tile, tile), :], tiles_ref.at[i], tile_sems.at[i]
         )
         for i in range(steps)
     ]
 
     @pl.when(step == 0)
     def fetch():
+        arriving = []
+        for j, kv_ref in enumerate(kv_refs):
+            arriving.append(
+                pltpu.make_async_copy(
+                    kv_ref.at[pl.ds(0, marked)], keys_ref.at[j, pl.ds(0, marked)], key_sems.at[j]
+                )
+            )
+        tiles_first = tiles[:1]
+        for j, kv_ref in enumerate(kv_refs):
+            for g in range(groups):
+                arriving.append(
+                    pltpu.make_async_copy(
+                        kv_ref.at[pl.ds(marked, HEAD), pl.ds(g * HEAD, HEAD)],
+                        values_ref.at[j, pl.ds(g * HEAD, HEAD)],
+                        value_sems.at[j * groups + g],
+                    )
+                )
+        for copy in tiles_first + arriving + tiles[1:]:
+            copy.start()
+        largest = jnp.max(jnp.abs(query_gain_ref[...])) * jnp.max(jnp.abs(key_gain_ref[...]))
+        small_ref[0] = (largest * (HEAD * score_scale * 1.02) < 50.0).astype(jnp.int32)
+        for j in range(SHARDS):
+            keys_ref[j, marked:, :] = jnp.zeros((depth - marked, tok_rows), bf16)
         for copy in arriving:
-            copy.start()
-
-
-    @pl.when(step == 0)
-    def fill():
-        for j in range(shards):
-            keys_ref[j, :marked, :] = kv_ref[j, :marked, :]
-            keys_ref[j, marked:, :] = jnp.zeros((depth - marked, tok_rows), bf16)
-            line = kv_ref[j, HEAD:marked, :].astype(f32)
+            copy.wait()
+        for j in range(SHARDS):
+            line = keys_ref[j, HEAD:marked, :].astype(f32)
             first_ref[j] = line[MARKS - 1, 0].astype(jnp.int32)
             last_ref[j] = line[MARKS - 1, tok_rows - 1].astype(jnp.int32)
 
     for i in range(steps):
-        pl.when(step == i)(arriving[i].wait)
+        pl.when(step == i)(tiles[i].wait)
     query_ref = tiles_ref.at[step]
     queries = query_ref[...].reshape(rows, depth)
-    top = query_ref[0, :16, HEAD:].astype(f32)
-    bottom = query_ref[0, tile - 16 :, HEAD:].astype(f32)
-    low = top[0, MARKS - 2].astype(jnp.int32)
-    high = bottom[15, MARKS - 2].astype(jnp.int32)
-    from_shard = jnp.int32(0)
-    to_shard = jnp.int32(0)
-    for j in range(shards):
-        from_shard += (last_ref[j] < low).astype(jnp.int32)
-        to_shard += (first_ref[j] <= high).astype(jnp.int32)
+    low = jnp.int32(1 << 20)
+    high = jnp.int32(-1)
+    half = all_rows // 2
+    for begin in range(0, tile, half):
+        top = query_ref[0, begin : begin + 16, HEAD:].astype(f32)
+        bottom = query_ref[0, begin + half - 16 : begin + half, HEAD:].astype(f32)
+        low = jnp.minimum(low, top[0, MARKS - 2].astype(jnp.int32))
+        high = jnp.maximum(high, bottom[15, MARKS - 2].astype(jnp.int32))
+    count = jnp.int32(0)
+    for j in range(SHARDS):
+        order_ref[count] = jnp.int32(j)
+        count += ((first_ref[j] <= high) & (last_ref[j] >= low)).astype(jnp.int32)
 
     acc_ref[...] = jnp.zeros_like(acc_ref)
     total_ref[...] = jnp.zeros_like(total_ref)
 
     def scores_of(j):
         return jnp.dot(queries, keys_ref[j], preferred_element_type=f32)
-
-    def values_of(j):
-        return jnp.concatenate(
-            [kv_ref[j, marked:, g * HEAD : (g + 1) * HEAD] for g in range(tok_rows // HEAD)],
-            axis=0,
-        )
 
     def folded(weights):
         part = weights[:, :LANES]
@@ -206,34 +246,45 @@
     def without_max():
         max_ref[...] = jnp.zeros_like(max_ref)
 
-        def advance(j, unused):
+        def advance(i, unused):
+            j = order_ref[i]
             weights = jnp.exp2(scores_of(j) * score_scale)
             total_ref[...] += folded(weights)
             acc_ref[...] += jnp.dot(
-                weights.astype(bf16), values_of(j), preferred_element_type=f32
+                weights.astype(bf16), values_ref[j], preferred_element_type=f32
             )
             return unused
 
-        lax.fori_loop(from_shard, to_shard, advance, 0)
+        lax.fori_loop(0, count, advance, 0)
 
     @pl.when(small_ref[0] == 0)
     def with_max():
         max_ref[...] = jnp.full_like(max_ref, -1e30)
 
-        def advance(j, unused):
-            scores = scores_of(j) * score_scale
-            old_max = max_ref[...]
-            new_max = jnp.maximum(old_max, jnp.max(scores, axis=1, keepdims=True))
-            weights = jnp.exp2(scores - new_max[:, :1])
-            rescale = jnp.exp2(old_max - new_max)
-            max_ref[...] = new_max
-            total_ref[...] = total_ref[...] * rescale + folded(weights)
-            acc_ref[...] = acc_ref[...] * rescale + jnp.dot(
-                weights.astype(bf16), values_of(j), preferred_element_type=f32
-            )
-            return unused
-
-        lax.fori_loop(from_shard, to_shard, advance, 0)
+        some_rows = 512
+
+        def advance(i, unused):
+            j = order_ref[i]
+
+            def some_of(r, unused):
+                mine = pl.ds(pl.multiple_of((r % (tile // some_rows)) * some_rows, some_rows), some_rows)
+                held = pl.ds(pl.multiple_of(r * some_rows, some_rows), some_rows)
+                part = query_ref[r // (tile // some_rows), mine, :]
+                scores = jnp.dot(part, keys_ref[j], preferred_element_type=f32) * score_scale
+                old_max = max_ref[held]
+                new_max = jnp.maximum(old_max, jnp.max(scores, axis=1, keepdims=True))
+                weights = jnp.exp2(scores - new_max[:, :1])
+                rescale = jnp.exp2(old_max - new_max)
+                max_ref[held] = new_max
+                total_ref[held] = total_ref[held] * rescale + folded(weights)
+                acc_ref[held] = acc_ref[held] * rescale + jnp.dot(
+                    weights.astype(bf16), values_ref[j], preferred_element_type=f32
+                )
+                return unused
+
+            return lax.fori_loop(0, rows // some_rows, some_of, unused)
+
+        lax.fori_loop(0, count, advance, 0)
 
     rows_out = LANES
     eye = lax.broadcasted_iota(jnp.int32, (rows_out, LANES), 0) == lax.broadcasted_iota(
@@ -245,9 +296,11 @@
             lanes = slice(h * HEAD, (h + 1) * HEAD)
             total = jnp.sum(total_ref[mine], axis=1, keepdims=True)
             some = total > 0.0
-            held = jnp.where(some, total, 1.0)
-            out_ref[i, :rows_out, lanes] = (acc_ref[mine] / held).astype(bf16)
-            level = jnp.where(some, max_ref[mine] + jnp.log2(held), -1e30)
+            kept = jnp.where(some, total, 1.0)
+            level = jnp.where(some, max_ref[mine] + jnp.log2(kept), -1e30)
+            share = 1.0 / kept
+            mixed = acc_ref[mine] * share
+            out_ref[i, :rows_out, lanes] = mixed.astype(bf16)
             flat = jnp.sum(jnp.where(eye, level, 0.0), axis=0, keepdims=True)
             top = flat.astype(bf16).astype(f32)
             rest = flat - top
@@ -280,7 +333,7 @@
     rows = LANES
     heads = width // HEAD
     levels = jnp.sum(part_ref[:, rows:, :].astype(f32), axis=1)
-    pieces = [levels[i * TP : (i + 1) * TP] for i in range(SHARE)]
+    pieces = [levels[i * TP : (i + 1) * TP] for i in range(sources // TP)]
     highest = pieces[0]
     for piece in pieces[1:]:
         highest = jnp.maximum(highest, piece)
@@ -303,7 +356,7 @@
     for t in range(TP):
         for h in range(heads):
             mixed = jnp.zeros((rows, HEAD), f32)
-            for i in range(SHARE):
+            for i in range(sources // TP):
                 source = i * TP + t
                 mixed = mixed + columns[h][:, source : source + 1] * part_ref[
                     source, :rows, h * HEAD : (h + 1) * HEAD
@@ -385,23 +438,30 @@
 
 
 def final_kernel(
-    returned_ref, target_ref, weight_ref, middle_ref, gain_ref, bias_ref, out_ref, routed_ref
+    returned_ref, target_ref, weight_ref, middle_ref, gain_ref, bias_ref, out_ref, rows_ref
 ):
+    chunk = 256
+    chunks = returned_ref.shape[0] // chunk
+    cut = returned_ref.shape[1]
+    some = chunk // PARTS
+    swap = swap_matrix(chunk)
+    for c in range(chunks):
+        sorted_rows = jnp.dot(
+            swap, returned_ref[c * chunk : (c + 1) * chunk, :], preferred_element_type=f32
+        ).astype(bf16)
+        for p in range(PARTS):
+            rows_ref[c * some : (c + 1) * some, p * cut : (p + 1) * cut] = sorted_rows[
+                p * some : (p + 1) * some
+            ]
     rows = middle_ref.shape[0]
-    all_rows, cut = returned_ref.shape
-    col = lax.broadcasted_iota(jnp.int32, (rows, all_rows), 1)
-    part = (col // CAPACITY) % PARTS
-    slot = (col // (CAPACITY * PARTS)) * CAPACITY + col % CAPACITY
-    for k in range(2):
-        hit = slot == target_ref[:, k : k + 1]
-        weight = weight_ref[:, k : k + 1]
-        for p in range(PARTS):
-            chosen = jnp.where(hit & (part == p), 1.0, 0.0).astype(bf16)
-            picked = jnp.dot(chosen, returned_ref[...], preferred_element_type=f32) * weight
-            lanes = slice(p * cut, (p + 1) * cut)
-            routed_ref[:, lanes] = picked if k == 0 else routed_ref[:, lanes] + picked
+    slot = lax.broadcasted_iota(jnp.int32, (rows, rows_ref.shape[0]), 1)
+    chosen = jnp.concatenate(
+        [jnp.where(slot == target_ref[:, k : k + 1], 1.0, 0.0) for k in range(2)], axis=0
+    ).astype(bf16)
+    picked = jnp.dot(chosen, rows_ref[...], preferred_element_type=f32)
+    routed = picked[:rows] * weight_ref[:, 0:1] + picked[rows:] * weight_ref[:, 1:2]
     out_ref[...] = layer_norm(
-        alpha_mix * middle_ref[...].astype(f32) + routed_ref[...], gain_ref[...], bias_ref[...]
+        alpha_mix * middle_ref[...].astype(f32) + routed, gain_ref[...], bias_ref[...]
     ).astype(bf16)
 
 
@@ -426,34 +486,87 @@
     return pltpu.CompilerParams(vmem_limit_bytes=mib << 20, **more)
 
 
-def attention_call(small, shared_rot, kv_all):
+def merge_kernel(own_any, other_any, out_hbm, own_ref, other_ref, out_ref, sems):
+    blocks = out_ref.shape[0]
+    rows = LANES
+    heads = out_ref.shape[2] // HEAD
+    arriving = [
+        pltpu.make_async_copy(own_any.at[pl.ds(blocks, blocks)], own_ref, sems.at[0]),
+        pltpu.make_async_copy(other_any.at[pl.ds(0, blocks)], other_ref, sems.at[1]),
+    ]
+    for copy in arriving:
+        copy.start()
+    for copy in arriving:
+        copy.wait()
+    flats = [
+        jnp.sum(ref[:, rows:, :].astype(f32), axis=1) for ref in (own_ref, other_ref)
+    ]
+    upper = jnp.maximum(flats[0], flats[1])
+    parts = [jnp.exp2(flat - upper) for flat in flats]
+    both = parts[0] + parts[1]
+    flat = upper + jnp.log2(both)
+    top = flat.astype(bf16).astype(f32)
+    rest = flat - top
+    middle = rest.astype(bf16).astype(f32)
+    final = rest - middle
+    for h in range(heads):
+        lanes = slice(h * HEAD, (h + 1) * HEAD)
+        shares = jnp.concatenate(
+            [(part / both)[:, lanes] for part in parts]
+            + [jnp.zeros((LANES - 2 * blocks, LANES), f32)],
+            axis=0,
+        )
+        columns = jnp.transpose(shares)
+        for i in range(blocks):
+            out_ref[i, :rows, lanes] = (
+                own_ref[i, :rows, lanes].astype(f32) * columns[:, i : i + 1]
+                + other_ref[i, :rows, lanes].astype(f32) * columns[:, blocks + i : blocks + i + 1]
+            ).astype(bf16)
+            out_ref[i, rows:, lanes] = jnp.concatenate(
+                [
+                    top[i : i + 1, lanes], middle[i : i + 1, lanes], final[i : i + 1, lanes],
+                    jnp.zeros((13, LANES), f32),
+                ],
+                axis=0,
+            ).astype(bf16)
+    leaving = pltpu.make_async_copy(out_ref, out_hbm, sems.at[2])
+    leaving.start()
+    leaving.wait()
+
+
+def attention_call(query_gain, key_gain, shared_rot, kv_parts):
     heads, all_rows, depth = shared_rot.shape
-    shards, _, tok_rows = kv_all.shape
+    tok_rows = kv_parts[0].shape[1]
     tile = TILE
     width = heads * HEAD
+    steps = all_rows // tile
+    out_block = pl.BlockSpec((tile // LANES, LANES + 16, width), lambda i: (i, 0, 0))
     return pl.pallas_call(
         attention_kernel,
-        grid=(all_rows // tile,),
-        out_shape=jax.ShapeDtypeStruct((all_rows // LANES, LANES + 16, width), bf16),
-        in_specs=[
-            in_smem(),
-            in_hbm(),
-            whole_vmem(),
-        ],
-        out_specs=pl.BlockSpec((tile // LANES, LANES + 16, width), lambda i: (i, 0, 0)),
+        grid=(steps,),
+        out_shape=pltpu.HBM((all_rows // LANES, LANES + 16, width), bf16),
+        in_specs=[whole_vmem(), whole_vmem(), in_hbm()] + [pl.BlockSpec(memory_space=pl.ANY)] * SHARDS,
+        out_specs=out_block,
         scratch_shapes=[
-            pltpu.VMEM((shards, depth, tok_rows), bf16),
-            pltpu.SMEM((shards,), jnp.int32),
-            pltpu.SMEM((shards,), jnp.int32),
+            pltpu.VMEM((SHARDS, depth, tok_rows), bf16),
+            pltpu.VMEM((SHARDS, tok_rows, HEAD), bf16),
+            pltpu.SMEM((SHARDS,), jnp.int32),
+            pltpu.SMEM((SHARDS,), jnp.int32),
+            pltpu.SMEM((SHARDS,), jnp.int32),
+            pltpu.SMEM((1,), jnp.int32),
             pltpu.VMEM((heads * tile, HEAD), f32),
             pltpu.VMEM((heads * tile, HEAD), f32),
             pltpu.VMEM((heads * tile, HEAD), f32),
-            pltpu.VMEM((all_rows // tile, heads, tile, depth), bf16),
-            pltpu.SemaphoreType.DMA((all_rows // tile,)),
+            pltpu.VMEM((steps, heads, tile, depth), bf16),
+            pltpu.SemaphoreType.DMA((steps,)),
+            pltpu.SemaphoreType.DMA((SHARDS,)),
+            pltpu.SemaphoreType.DMA((SHARDS * tok_rows // HEAD,)),
         ],
         compiler_params=params(40, 1),
         name="document_attention",
-    )(small, held(shared_rot), kv_all)
+    )(
+        query_gain.reshape(1, HEAD), key_gain.reshape(1, HEAD), held(shared_rot), *kv_parts,
+    )
 
 
 def per_device(
@@ -468,18 +581,21 @@
     shards = sp_size // SHARE
     table = jnp.asarray(angle_tables(sp_size * tok_rows // GRID))
     index = lax.axis_index("sp").astype(jnp.int32).reshape(1)
-    class_groups = [[c + SHARE * j for j in range(shards)] for c in range(SHARE)]
     owner_groups = [
-        [(g * SHARE + i) * tp_size + t for i in range(SHARE) for t in range(tp_size)]
+        [(g * SHARE + c + 2 * i) * tp_size + t for i in range(SHARE // 2) for t in range(tp_size)]
         for g in range(shards)
+        for c in range(2)
     ]
 
     kv_rows = 2 * HEAD + MARKS
-    kv = pl.pallas_call(
+    kv, marked = pl.pallas_call(
         key_kernel,
-        out_shape=pltpu.HBM((shards, kv_rows, tok_rows), bf16),
-        in_specs=[in_smem()] + [in_hbm()] * 5,
-        out_specs=in_hbm(),
+        out_shape=(
+            pltpu.HBM((kv_rows, tok_rows), bf16),
+            pltpu.HBM((tok_rows + MARKS, width), bf16),
+        ),
+        in_specs=[in_smem()] + [in_hbm()] * 6,
+        out_specs=(in_hbm(), in_hbm()),
         scratch_shapes=[
             pltpu.VMEM(key_heads.shape, bf16),
             pltpu.VMEM(value_heads.shape, bf16),
@@ -487,41 +603,75 @@
             pltpu.VMEM((1, HEAD), f32),
             pltpu.VMEM(table.shape, f32),
             pltpu.VMEM((kv_rows, tok_rows), bf16),
-            pltpu.SemaphoreType.DMA((5,)),
-            pltpu.SemaphoreType.DMA((shards,)),
+            pltpu.VMEM((tok_rows + MARKS, width), bf16),
+            pltpu.SemaphoreType.DMA((6,)),
+            pltpu.SemaphoreType.DMA((2,)),
         ],
         compiler_params=params(16),
         name="key_rotation",
     )(
         index, held(key_heads), held(value_heads), held(documents.reshape(1, tok_rows)),
-        held(key_gain.reshape(1, HEAD)), held(table),
-    )
-    kv_all = lax.all_to_all(kv, "sp", 0, 0, tiled=True, axis_index_groups=class_groups)
-
-    lines = documents.astype(bf16).reshape(tok_rows // width, width)
-    marked = jnp.concatenate(
-        [queries, lines, jnp.zeros((MARKS - tok_rows // width, width), bf16)], axis=0
-    )
+        held(key_gain.reshape(1, HEAD)), held(table), held(queries),
+    )
+
+    def moved(array, dz, dy):
+        pairs = []
+        for z in range(4):
+            for y in range(4):
+                for c in range(2):
+                    way = 1 - 2 * c
+                    goal = ((z + way * dz) % 4) * 8 + ((y + way * dy) % 4) * 2 + c
+                    pairs.append((z * 8 + y * 2 + c, goal))
+        return lax.ppermute(array, "sp", pairs)
+
+    across = moved(kv, 0, 2)
+    after = moved(kv, 1, 0)
+    ahead = moved(kv, -1, 0)
+    beyond = moved(after, 1, 0)
+    after_across = moved(across, 1, 0)
+    ahead_across = moved(across, -1, 0)
+    beyond_across = moved(after_across, 1, 0)
+    kv_parts = [kv, after, ahead, across, beyond, after_across, ahead_across, beyond_across]
+
+    beside = lax.ppermute(marked, "sp", [(i, i ^ 2) for i in range(sp_size)])
     shared = [marked]
-    for k in range(1, SHARE):
-        shared.append(lax.ppermute(marked, "sp", [(i, i ^ k) for i in range(sp_size)]))
+    for array in (marked, beside):
+        shared.append(lax.ppermute(array, "sp", [(i, i ^ 1) for i in range(sp_size)]))
+    shared.insert(2, beside)
 
     shared_rot = pl.pallas_call(
         query_kernel,
         out_shape=pltpu.HBM((heads, SHARE * tok_rows, 2 * HEAD), bf16),
-        in_specs=[in_smem()] + [whole_vmem()] * (SHARE + 2),
+        in_specs=[in_smem()] + [pl.BlockSpec(memory_space=pl.ANY)] * SHARE + [in_hbm()] * 2,
         out_specs=in_hbm(),
         scratch_shapes=[
             pltpu.VMEM((heads, SHARE * tok_rows, 2 * HEAD), bf16),
+            pltpu.VMEM((1, HEAD), f32),
+            pltpu.VMEM(table.shape, f32),
+            pltpu.VMEM((SHARE,) + marked.shape, bf16),
             pltpu.SemaphoreType.DMA((heads,)),
+            pltpu.SemaphoreType.DMA((2 + SHARE,)),
         ],
         compiler_params=params(24),
         name="query_rotation",
-    )(index, *shared, query_gain.reshape(1, HEAD), table)
-
-    largest = jnp.max(jnp.abs(query_gain)) * jnp.max(jnp.abs(key_gain))
-    small = (largest * (HEAD * score_scale * 1.02) < 50.0).astype(jnp.int32).reshape(1)
-    partial = attention_call(small, shared_rot, kv_all)
+    )(index, held(marked), *shared[1:], held(query_gain.reshape(1, HEAD)), held(table))
+
+    partial = attention_call(query_gain, key_gain, shared_rot, kv_parts)
+    other = lax.ppermute(partial, "sp", [(i, i ^ 1) for i in range(sp_size)])
+    blocks = partial.shape[0] // 2
+    block = (blocks,) + partial.shape[1:]
+    partial = pl.pallas_call(
+        merge_kernel,
+        out_shape=pltpu.HBM(block, bf16),
+        in_specs=[pl.BlockSpec(memory_space=pl.ANY)] * 2,
+        out_specs=in_hbm(),
+        scratch_shapes=[
+            pltpu.VMEM(block, bf16), pltpu.VMEM(block, bf16), pltpu.VMEM(block, bf16),
+            pltpu.SemaphoreType.DMA((3,)),
+        ],
+        compiler_params=params(16),
+        name="merge_parts",
+    )(held(partial), other)
     partial = lax.all_to_all(
         partial, ("sp", "tp"), 0, 0, tiled=True, axis_index_groups=owner_groups
     )
@@ -586,7 +736,7 @@
         out_shape=jax.ShapeDtypeStruct((out_rows, model_width), bf16),
         in_specs=[whole_vmem() for _ in range(6)],
         out_specs=whole_vmem(),
-        scratch_shapes=[pltpu.VMEM((out_rows, model_width), f32)],
+        scratch_shapes=[pltpu.VMEM((expert_total * CAPACITY, model_width), bf16)],
         compiler_params=params(40),
         name="final_stream",
     )(

time: 195 us -> 198 us (1.015)
  waiting for transfers between devices: 78.9 us -> 56.7 us
  Pallas kernels: 50.6 us -> 63.8 us
  starting transfers between devices: 24.4 us -> 33.9 us
  blocking collectives: 36.8 us -> 42.7 us
    ppermute x3 -> x11, starting transfers between devices: 2.76 us -> 25.9 us  [the longest x7 15.7 us: moved(): return lax.ppermute(array, 'sp', pairs)]
    ppermute x3 -> x11, waiting for transfers between devices: 31.8 us -> 15.3 us  [the longest x1 5.65 us: per_device(): beside = lax.ppermute(marked, 'sp', [(i, i ^ 2) for i in range(sp_size)])]
    pallas_call x2 -> x3, Pallas kernels: 32 us -> 46.3 us  [the longest x1 41.2 us: attention_call(): pl.pallas_call(attention_kernel, grid=(steps,), out_shape=pltpu.HBM((all_...]
    all_to_all x1 -> x0, starting transfers between devices: 8.63 us -> none  [per_device(): lax.all_to_all(kv, 'sp', 0, 0, tiled=True, axis_index_groups=class_groups)]
    all_to_all x1, blocking collectives: 36.8 us -> 42.7 us  [per_device(): lax.all_to_all(outbound.reshape(expert_total, CAPACITY * PARTS, cut), ('s...]
    all_to_all x1, waiting for transfers between devices: 16.4 us -> 10.6 us  [per_device(): lax.all_to_all(partial, ('sp', 'tp'), 0, 0, tiled=True, axis_index_groups...]
    all_to_all x1, starting transfers between devices: 9.05 us -> 4.03 us  [per_device(): lax.all_to_all(partial, ('sp', 'tp'), 0, 0, tiled=True, axis_index_groups...]
  transfers between devices with their start and end apart: 6 -> 13, of which waited for: 4 -> 7; matrix products, arithmetic and copies ran while one was open for 1% -> 0% of each run, Pallas kernels for 2% -> 2%
where the time goes in v2:
time: 198 us
  Pallas kernels  63.8 us (32%)
  waiting for transfers between devices  56.7 us (29%)
  blocking collectives  42.7 us (22%)
  starting transfers between devices  33.9 us (17%)
    all_to_all x1, blocking collectives, per_device(): lax.all_to_all(outbound.reshape(expert_total, CAPACITY * PARTS, cut), ('s...  42.7 us
    pallas_call x1, Pallas kernels, attention_call(): pl.pallas_call(attention_kernel, grid=(steps,), out_shape=pltpu.HBM((all_...  41.2 us
    all_to_all x1, waiting for transfers between devices, per_device(): lax.all_to_all(served.reshape(expert_total, CAPACITY * PARTS, cut), ('sp'...  30.8 us
    ppermute x7, starting transfers between devices, moved(): return lax.ppermute(array, 'sp', pairs)  15.7 us
    all_to_all x1, waiting for transfers between devices, per_device(): lax.all_to_all(partial, ('sp', 'tp'), 0, 0, tiled=True, axis_index_groups...  10.6 us
    ppermute x1, starting transfers between devices, per_device(): other = lax.ppermute(partial, 'sp', [(i, i ^ 1) for i in range(sp_size)])  8.96 us
    pallas_call x1, Pallas kernels, per_device(): pl.pallas_call(expert_kernel, out_shape=jax.ShapeDtypeStruct((exchange_ro...  5.93 us
    ppermute x1, waiting for transfers between devices, per_device(): beside = lax.ppermute(marked, 'sp', [(i, i ^ 2) for i in range(sp_size)])  5.65 us
  transfers between devices with their start and end apart: 13, of which 7 were waited for; matrix products, arithmetic and copies ran while one was open for 0% of the time, Pallas kernels for 2%

profile of v2, /device:TPU:1, one launch (start us, length us, event | category | flops | bytes accessed | tf_op | source)
XLA Modules:
  0.0 198.0 jit_solution(14372610137275216168)
XLA Ops:
  0.0 0.0 copy-start.10
  0.0 0.0 copy-start.11
  0.0 2.3 %key_rotation.1 = (bf16[272,512]{1,0:T(8,128)(2,1)}, bf16[528,256]{1,0:T(8,128)(2,1)}) custom-call(s32[1]{0:T(128)} %bitcast.2.index_ref, bf16[512,128]{1,0:T(8,128)(2,1)} %key_hbm.1, bf16[512,128]{1,0:T(8,128)(2,1)} %value_hbm.1, s32[1,512]{1,0:T(1,128)} %bitcast.46, f32[1,128]{1,0:T(1,128)} %bitcast.41, f32[640,128]{1,0:T(8,128)} %constant.12.clone.table_hbm.refs_5_, ...), custom_call_target="tpu_custom_call" | custom-call | tf_op jit(solution)/shard_map/key_rotation/pallas_call | solution.py:591
  2.3 0.0 copy-start.4
  2.4 3.8 %collective-permute-start.5 = (bf16[272,512]{1,0:T(8,128)(2,1)}, bf16[272,512]{1,0:T(8,128)(2,1)S(1)}, u32[]{:S(2)}, u32[]{:S(2)}) collective-permute-start(bf16[272,512]{1,0:T(8,128)(2,1)} %get-tuple-element.10.refs_0_), channel_id=1, source_target_pairs={{0,16},{4,20},{8,24},{12,28},{16,0},{20,4},{24,8},{28,12},{32,48},... | collective-permute-start | bytes 835592 | tf_op jit(solution)/shard_map/ppermute | solution.py:625
  6.2 3.8 %collective-permute-start.3 = (bf16[272,512]{1,0:T(8,128)(2,1)}, bf16[272,512]{1,0:T(8,128)(2,1)S(1)}, u32[]{:S(2)}, u32[]{:S(2)}) collective-permute-start(bf16[272,512]{1,0:T(8,128)(2,1)} %get-tuple-element.10.refs_0_), channel_id=1, source_target_pairs={{0,32},{4,100},{8,40},{12,108},{16,48},{20,116},{24,56},{28,124},{... | collective-permute-start | bytes 835592 | tf_op jit(solution)/shard_map/ppermute | solution.py:625
  9.9 2.6 %collective-permute-done.5.refs_3_ = bf16[272,512]{1,0:T(8,128)(2,1)S(1)} collective-permute-done((bf16[272,512]{1,0:T(8,128)(2,1)}, bf16[272,512]{1,0:T(8,128)(2,1)S(1)}, u32[]{:S(2)}, u32[]{:S(2)}) %collective-permute-start.5) | collective-permute-done | bytes 278560 | tf_op jit(solution)/shard_map/ppermute | solution.py:625
  12.5 3.7 %collective-permute-start.7 = (bf16[272,512]{1,0:T(8,128)(2,1)S(1)}, bf16[272,512]{1,0:T(8,128)(2,1)S(1)}, u32[]{:S(2)}, u32[]{:S(2)}) collective-permute-start(bf16[272,512]{1,0:T(8,128)(2,1)S(1)} %collective-permute-done.5.refs_3_), channel_id=1, source_target_pairs={{0,32},{4,100},{8,40},{12,108},{16,48},{20,116},{24,56},{28,124},{... | collective-permute-start | bytes 835592 | tf_op jit(solution)/shard_map/ppermute | solution.py:625
  16.3 1.3 collective-permute-start.1
  17.6 0.0 collective-permute-start
  17.6 1.6 collective-permute-start.4
  19.2 5.7 %collective-permute-done.1.refs_2_ = bf16[528,256]{1,0:T(8,128)(2,1)S(1)} collective-permute-done((bf16[528,256]{1,0:T(8,128)(2,1)}, bf16[528,256]{1,0:T(8,128)(2,1)S(1)}, u32[]{:S(2)}, u32[]{:S(2)}) %collective-permute-start.1) | collective-permute-done | bytes 270368 | tf_op jit(solution)/shard_map/ppermute | solution.py:636
  24.8 0.0 collective-permute-start.8
  24.8 0.0 collective-permute-done.3.refs_1_
  24.8 2.7 %collective-permute-start.6 = (bf16[272,512]{1,0:T(8,128)(2,1)S(1)}, bf16[272,512]{1,0:T(8,128)(2,1)S(1)}, u32[]{:S(2)}, u32[]{:S(2)}) collective-permute-start(bf16[272,512]{1,0:T(8,128)(2,1)S(1)} %collective-permute-done.3.refs_1_), channel_id=1, source_target_pairs={{0,32},{4,100},{8,40},{12,108},{16,48},{20,116},{24,56},{28,124},{... | collective-permute-start | bytes 835592 | tf_op jit(solution)/shard_map/ppermute | solution.py:625
  27.5 0.0 collective-permute-done.7.refs_5_
  27.5 0.1 collective-permute-start.9
  27.6 0.0 collective-permute-done.refs_1_
  27.6 0.0 collective-permute-start.2
  27.6 1.5 collective-permute-done.2.refs_3_
  29.1 4.3 %query_rotation.1.query_hbm = bf16[2,2048,256]{2,1,0:T(8,128)(2,1)} custom-call(s32[1]{0:T(128)} %bitcast.2.index_ref, bf16[528,256]{1,0:T(8,128)(2,1)} %get-tuple-element.9.refs_0_, bf16[528,256]{1,0:T(8,128)(2,1)S(1)} %collective-permute-done.refs_1_, bf16[528,256]{1,0:T(8,128)(2,1)S(1)} %collective-permute-done.1.refs_2_, ...), custom_call_target="tpu_custom_call" | custom-call | tf_op jit(solution)/shard_map/query_rotation/pallas_call | solution.py:642
  33.4 0.0 copy-start.12
  33.4 0.0 collective-permute-done.4.refs_2_
  33.4 0.0 collective-permute-done.8.refs_6_
  33.4 0.0 collective-permute-done.6.refs_4_
  33.5 3.0 %collective-permute-done.9.refs_7_ = bf16[272,512]{1,0:T(8,128)(2,1)S(1)} collective-permute-done((bf16[272,512]{1,0:T(8,128)(2,1)S(1)}, bf16[272,512]{1,0:T(8,128)(2,1)S(1)}, u32[]{:S(2)}, u32[]{:S(2)}) %collective-permute-start.9) | collective-permute-done | bytes 278560 | tf_op jit(solution)/shard_map/ppermute | solution.py:625
  36.5 0.0 copy-done.10
  36.5 0.0 copy-done.11
  36.5 0.0 copy-done.4
  36.5 41.2 %document_attention.1.own_any = bf16[16,144,256]{2,1,0:T(8,128)(2,1)} custom-call(f32[1,128]{1,0:T(1,128)S(1)} %bitcast.40, f32[1,128]{1,0:T(1,128)S(1)} %bitcast.42, bf16[2,2048,256]{2,1,0:T(8,128)(2,1)} %query_rotation.1.query_hbm, bf16[272,512]{1,0:T(8,128)(2,1)S(1)} %copy-done.4, bf16[272,512]{1,0:T(8,128)(2,1)S(1)} %collective-permute-done.3.refs_1_, ...), custom_call_target="tpu_custom_call" | custom-call | tf_op jit(solution)/shard_map/document_attention/pallas_call | solution.py:544
  77.7 9.0 %collective-permute-start.10 = (bf16[16,144,256]{2,1,0:T(8,128)(2,1)}, bf16[16,144,256]{2,1,0:T(8,128)(2,1)S(1)}, u32[]{:S(2)}, u32[]{:S(2)}) collective-permute-start(bf16[16,144,256]{2,1,0:T(8,128)(2,1)} %document_attention.1.own_any), channel_id=1, source_target_pairs={{0,4},{4,0},{8,12},{12,8},{16,20},{20,16},{24,28},{28,24},{32,36},... | collective-permute-start | bytes 3538952 | tf_op jit(solution)/shard_map/ppermute | solution.py:660
  86.7 0.0 copy-done.12
  86.7 0.1 copy.33
  86.8 0.1 copy.35
  86.8 0.0 copy-start.3
  86.8 0.0 copy-start.5
  86.9 0.0 copy-start.9
  86.9 2.5 %collective-permute-done.10.other_any = bf16[16,144,256]{2,1,0:T(8,128)(2,1)S(1)} collective-permute-done((bf16[16,144,256]{2,1,0:T(8,128)(2,1)}, bf16[16,144,256]{2,1,0:T(8,128)(2,1)S(1)}, u32[]{:S(2)}, u32[]{:S(2)}) %collective-permute-start.10) | collective-permute-done | bytes 1179680 | tf_op jit(solution)/shard_map/ppermute | solution.py:660
  89.4 2.8 %merge_parts.1 = bf16[8,144,256]{2,1,0:T(8,128)(2,1)} custom-call(bf16[16,144,256]{2,1,0:T(8,128)(2,1)} %document_attention.1.own_any, bf16[16,144,256]{2,1,0:T(8,128)(2,1)S(1)} %collective-permute-done.10.other_any), custom_call_target="tpu_custom_call" | custom-call | tf_op jit(solution)/shard_map/merge_parts/pallas_call | solution.py:663
  92.2 4.0 %all-to-all-start = ((bf16[8,144,256]{2,1,0:T(8,128)(2,1)}), bf16[8,144,256]{2,1,0:T(8,128)(2,1)S(1)}, u32[]{:S(2)}, u32[]{:S(2)}) async-start(bf16[8,144,256]{2,1,0:T(8,128)(2,1)} %merge_parts.1), calls=%async_computation | async-start | bytes 1179648 | tf_op jit(solution)/shard_map/all_to_all | solution.py:675
  96.2 0.2 convert_reduce_fusion
  96.4 0.1 copy.36
  96.5 0.1 copy.37
  96.6 10.6 %all-to-all-done.part_ref = bf16[8,144,256]{2,1,0:T(8,128)(2,1)S(1)} async-done(((bf16[8,144,256]{2,1,0:T(8,128)(2,1)}), bf16[8,144,256]{2,1,0:T(8,128)(2,1)S(1)}, u32[]{:S(2)}, u32[]{:S(2)}) %all-to-all-start) | async-done | bytes 589856 | tf_op jit(solution)/shard_map/all_to_all | solution.py:675
  107.1 0.0 copy-done.3
  107.1 0.0 copy-done.5
  107.1 0.0 copy-done.6
  107.1 0.0 copy-done.9
  107.2 0.0 copy-start.2
  107.2 4.8 %middle_stream.1 = (bf16[128,2048]{1,0:T(8,128)(2,1)S(1)}, bf16[2048,512]{1,0:T(8,128)(2,1)S(1)}) custom-call(bf16[8,144,256]{2,1,0:T(8,128)(2,1)S(1)} %all-to-all-done.part_ref, f32[1,1024]{1,0:T(1,128)S(1)} %bitcast.38, bf16[1024,2048]{1,0:T(8,128)(2,1)} %proj_ref.1, bf16[128,2048]{1,0:T(8,128)(2,1)S(1)} %copy-done.3, f32[1,2048]{1,0:T(1,128)S(1)} %bitcast.34, ...), custom_call_target="tpu_custom_call" | custom-call | tf_op jit(solution)/shard_map/middle_stream/pallas_call | solution.py:689
  112.0 0.0 copy-start
  112.0 0.0 copy-start.1
  112.0 42.7 %all_to_all.15 = bf16[128,16,512]{2,1,0:T(8,128)(2,1)S(1)} all-to-all(bf16[128,16,512]{2,1,0:T(8,128)(2,1)S(1)} %bitcast.31), channel_id=1, replica_groups=mesh['sp'=32,'tp'=4] {'sp','tp'}, dimensions={0} | all-to-all | bytes 4194304 | tf_op jit(solution)/shard_map/all_to_all | solution.py:710
  154.8 0.0 copy-done.2
  154.8 0.0 copy-done
  154.8 0.0 copy-done.1
  154.8 5.9 %expert.1 = bf16[2048,512]{1,0:T(8,128)(2,1)} custom-call(bf16[2048,512]{1,0:T(8,128)(2,1)S(1)} %bitcast.26, bf16[2048,512]{1,0:T(8,128)(2,1)S(1)} %bitcast.28, bf16[2048,512]{1,0:T(8,128)(2,1)S(1)} %bitcast.29, bf16[512,2048]{1,0:T(8,128)(2,1)S(1)} %bitcast.30), custom_call_target="tpu_custom_call" | custom-call | tf_op jit(solution)/shard_map/expert/pallas_call | solution.py:714
  160.7 3.9 %all-to-all-start.2 = ((bf16[128,16,512]{2,1,0:T(8,128)(2,1)}), bf16[128,16,512]{2,1,0:T(8,128)(2,1)S(1)}, u32[]{:S(2)}, u32[]{:S(2)}) async-start(bf16[128,16,512]{2,1,0:T(8,128)(2,1)} %bitcast.15), calls=%async_computation.2 | async-start | bytes 4194304 | tf_op jit(solution)/shard_map/all_to_all | solution.py:731
  164.7 0.0 copy-done.13
  164.7 0.1 copy.38.weight_ref
  164.8 30.8 %all-to-all-done.2 = bf16[128,16,512]{2,1,0:T(8,128)(2,1)S(1)} async-done(((bf16[128,16,512]{2,1,0:T(8,128)(2,1)}), bf16[128,16,512]{2,1,0:T(8,128)(2,1)S(1)}, u32[]{:S(2)}, u32[]{:S(2)}) %all-to-all-start.2) | async-done | bytes 2097184 | tf_op jit(solution)/shard_map/all_to_all | solution.py:731
  195.6 0.0 copy-done.7
  195.6 0.0 copy-done.8
  195.6 2.4 %final_stream.1 = bf16[128,2048]{1,0:T(8,128)(2,1)} custom-call(bf16[2048,512]{1,0:T(8,128)(2,1)S(1)} %bitcast.27, s32[128,2]{1,0:T(8,128)S(1)} %bitcast.32, f32[128,2]{1,0:T(8,128)S(1)} %copy.38.weight_ref, bf16[128,2048]{1,0:T(8,128)(2,1)S(1)} %get-tuple-element.12.middle_ref, f32[1,2048]{1,0:T(1,128)S(1)} %bitcast.36, f32[1,2048]{1,0:T(1,128)S(1)} %bitcast.37), custom_call_target="tpu_custom_call" | custom-call | tf_op jit(solution)/shard_map/final_stream/pallas_call | solution.py:734
  (7 shorter events, 0.0 us)
Async XLA Ops:
  0.0 36.5 %copy-start.10 = (f32[128]{0:T(128)S(1)}, f32[128]{0:T(128)}, u32[]{:S(2)}) copy-start(f32[128]{0:T(128)} %param.23) | copy-start | bytes 1540
  0.0 36.5 %copy-start.11 = (f32[128]{0:T(128)S(1)}, f32[128]{0:T(128)}, u32[]{:S(2)}) copy-start(f32[128]{0:T(128)} %param.24) | copy-start | bytes 1540
  2.3 34.2 %copy-start.4 = (bf16[272,512]{1,0:T(8,128)(2,1)S(1)}, bf16[272,512]{1,0:T(8,128)(2,1)}, u32[]{:S(2)}) copy-start(bf16[272,512]{1,0:T(8,128)(2,1)} %get-tuple-element.10.refs_0_) | copy-start | bytes 835588
  2.4 10.2 %collective-permute-start.5 = (bf16[272,512]{1,0:T(8,128)(2,1)}, bf16[272,512]{1,0:T(8,128)(2,1)S(1)}, u32[]{:S(2)}, u32[]{:S(2)}) collective-permute-start(bf16[272,512]{1,0:T(8,128)(2,1)} %get-tuple-element.10.refs_0_), channel_id=1, source_target_pairs={{0,16},{4,20},{8,24},{12,28},{16,0},{20,4},{24,8},{28,12},{32,48},... | collective-permute-start | bytes 835592 | tf_op jit(solution)/shard_map/ppermute | solution.py:625
  6.2 18.7 %collective-permute-start.3 = (bf16[272,512]{1,0:T(8,128)(2,1)}, bf16[272,512]{1,0:T(8,128)(2,1)S(1)}, u32[]{:S(2)}, u32[]{:S(2)}) collective-permute-start(bf16[272,512]{1,0:T(8,128)(2,1)} %get-tuple-element.10.refs_0_), channel_id=1, source_target_pairs={{0,32},{4,100},{8,40},{12,108},{16,48},{20,116},{24,56},{28,124},{... | collective-permute-start | bytes 835592 | tf_op jit(solution)/shard_map/ppermute | solution.py:625
  12.5 15.0 %collective-permute-start.7 = (bf16[272,512]{1,0:T(8,128)(2,1)S(1)}, bf16[272,512]{1,0:T(8,128)(2,1)S(1)}, u32[]{:S(2)}, u32[]{:S(2)}) collective-permute-start(bf16[272,512]{1,0:T(8,128)(2,1)S(1)} %collective-permute-done.5.refs_3_), channel_id=1, source_target_pairs={{0,32},{4,100},{8,40},{12,108},{16,48},{20,116},{24,56},{28,124},{... | collective-permute-start | bytes 835592 | tf_op jit(solution)/shard_map/ppermute | solution.py:625
  16.3 8.6 %collective-permute-start.1 = (bf16[528,256]{1,0:T(8,128)(2,1)}, bf16[528,256]{1,0:T(8,128)(2,1)S(1)}, u32[]{:S(2)}, u32[]{:S(2)}) collective-permute-start(bf16[528,256]{1,0:T(8,128)(2,1)} %get-tuple-element.9.refs_0_), channel_id=1, source_target_pairs={{0,8},{4,12},{8,0},{12,4},{16,24},{20,28},{24,16},{28,20},{32,40},... | collective-permute-start | bytes 811016 | tf_op jit(solution)/shard_map/ppermute | solution.py:636
  17.6 10.0 %collective-permute-start = (bf16[528,256]{1,0:T(8,128)(2,1)}, bf16[528,256]{1,0:T(8,128)(2,1)S(1)}, u32[]{:S(2)}, u32[]{:S(2)}) collective-permute-start(bf16[528,256]{1,0:T(8,128)(2,1)} %get-tuple-element.9.refs_0_), channel_id=1, source_target_pairs={{0,4},{4,0},{8,12},{12,8},{16,20},{20,16},{24,28},{28,24},{32,36},... | collective-permute-start | bytes 811016 | tf_op jit(solution)/shard_map/ppermute | solution.py:639
  17.6 15.9 %collective-permute-start.4 = (bf16[272,512]{1,0:T(8,128)(2,1)}, bf16[272,512]{1,0:T(8,128)(2,1)S(1)}, u32[]{:S(2)}, u32[]{:S(2)}) collective-permute-start(bf16[272,512]{1,0:T(8,128)(2,1)} %get-tuple-element.10.refs_0_), channel_id=1, source_target_pairs={{0,96},{4,36},{8,104},{12,44},{16,112},{20,52},{24,120},{28,60},{3... | collective-permute-start | bytes 835592 | tf_op jit(solution)/shard_map/ppermute | solution.py:625
  24.8 8.6 %collective-permute-start.8 = (bf16[272,512]{1,0:T(8,128)(2,1)S(1)}, bf16[272,512]{1,0:T(8,128)(2,1)S(1)}, u32[]{:S(2)}, u32[]{:S(2)}) collective-permute-start(bf16[272,512]{1,0:T(8,128)(2,1)S(1)} %collective-permute-done.5.refs_3_), channel_id=1, source_target_pairs={{0,96},{4,36},{8,104},{12,44},{16,112},{20,52},{24,120},{28,60},{3... | collective-permute-start | bytes 835592 | tf_op jit(solution)/shard_map/ppermute | solution.py:625
  24.8 8.6 %collective-permute-start.6 = (bf16[272,512]{1,0:T(8,128)(2,1)S(1)}, bf16[272,512]{1,0:T(8,128)(2,1)S(1)}, u32[]{:S(2)}, u32[]{:S(2)}) collective-permute-start(bf16[272,512]{1,0:T(8,128)(2,1)S(1)} %collective-permute-done.3.refs_1_), channel_id=1, source_target_pairs={{0,32},{4,100},{8,40},{12,108},{16,48},{20,116},{24,56},{28,124},{... | collective-permute-start | bytes 835592 | tf_op jit(solution)/shard_map/ppermute | solution.py:625
  27.5 9.0 %collective-permute-start.9 = (bf16[272,512]{1,0:T(8,128)(2,1)S(1)}, bf16[272,512]{1,0:T(8,128)(2,1)S(1)}, u32[]{:S(2)}, u32[]{:S(2)}) collective-permute-start(bf16[272,512]{1,0:T(8,128)(2,1)S(1)} %collective-permute-done.7.refs_5_), channel_id=1, source_target_pairs={{0,32},{4,100},{8,40},{12,108},{16,48},{20,116},{24,56},{28,124},{... | collective-permute-start | bytes 835592 | tf_op jit(solution)/shard_map/ppermute | solution.py:625
  27.6 1.6 collective-permute-start.2
  33.4 53.3 %copy-start.12 = (s32[128,2]{0,1:T(2,128)S(1)}, s32[128,2]{0,1:T(2,128)}, u32[]{:S(2)}) copy-start(s32[128,2]{0,1:T(2,128)} %param.30) | copy-start | bytes 3076
  77.7 11.6 %collective-permute-start.10 = (bf16[16,144,256]{2,1,0:T(8,128)(2,1)}, bf16[16,144,256]{2,1,0:T(8,128)(2,1)S(1)}, u32[]{:S(2)}, u32[]{:S(2)}) collective-permute-start(bf16[16,144,256]{2,1,0:T(8,128)(2,1)} %document_attention.1.own_any), channel_id=1, source_target_pairs={{0,4},{4,0},{8,12},{12,8},{16,20},{20,16},{24,28},{28,24},{32,36},... | collective-permute-start | bytes 3538952 | tf_op jit(solution)/shard_map/ppermute | solution.py:660
  86.8 20.3 %copy-start.3 = (bf16[128,2048]{1,0:T(8,128)(2,1)S(1)}, bf16[128,2048]{1,0:T(8,128)(2,1)}, u32[]{:S(2)}) copy-start(bf16[128,2048]{1,0:T(8,128)(2,1)} %residual_ref.1) | copy-start | bytes 1572868
  86.8 20.3 %copy-start.5 = (f32[2048]{0:T(1024)S(1)}, f32[2048]{0:T(1024)}, u32[]{:S(2)}) copy-start(f32[2048]{0:T(1024)} %param.28) | copy-start | bytes 24580
  86.9 20.3 %copy-start.6 = (f32[2048]{0:T(1024)S(1)}, f32[2048]{0:T(1024)}, u32[]{:S(2)}) copy-start(f32[2048]{0:T(1024)} %param.29) | copy-start | bytes 24580
  86.9 20.3 %copy-start.9 = (f32[1024]{0:T(1024)S(1)}, f32[1024]{0:T(1024)}, u32[]{:S(2)}) copy-start(f32[1024]{0:T(1024)} %param.25) | copy-start | bytes 12292
  92.2 15.0 %all-to-all-start = ((bf16[8,144,256]{2,1,0:T(8,128)(2,1)}), bf16[8,144,256]{2,1,0:T(8,128)(2,1)S(1)}, u32[]{:S(2)}, u32[]{:S(2)}) async-start(bf16[8,144,256]{2,1,0:T(8,128)(2,1)} %merge_parts.1), calls=%async_computation | async-start | bytes 1179648 | tf_op jit(solution)/shard_map/all_to_all | solution.py:675
  107.2 47.6 %copy-start.2 = (bf16[1,512,2048]{2,1,0:T(8,128)(2,1)S(1)}, bf16[1,512,2048]{2,1,0:T(8,128)(2,1)}, u32[]{:S(2)}) copy-start(bf16[1,512,2048]{2,1,0:T(8,128)(2,1)} %param.34) | copy-start | bytes 6291460
  112.0 42.8 %copy-start = (bf16[1,2048,512]{2,1,0:T(8,128)(2,1)S(1)}, bf16[1,2048,512]{2,1,0:T(8,128)(2,1)}, u32[]{:S(2)}) copy-start(bf16[1,2048,512]{2,1,0:T(8,128)(2,1)} %param.32) | copy-start | bytes 6291460
  112.0 42.8 %copy-start.1 = (bf16[1,2048,512]{2,1,0:T(8,128)(2,1)S(1)}, bf16[1,2048,512]{2,1,0:T(8,128)(2,1)}, u32[]{:S(2)}) copy-start(bf16[1,2048,512]{2,1,0:T(8,128)(2,1)} %param.33) | copy-start | bytes 6291460
  160.7 3.9 %copy-start.13 = (f32[128,2]{0,1:T(2,128)S(1)}, f32[128,2]{0,1:T(2,128)}, u32[]{:S(2)}) copy-start(f32[128,2]{0,1:T(2,128)} %param.31) | copy-start | bytes 3076
  160.7 34.8 %copy-start.7 = (f32[2048]{0:T(1024)S(1)}, f32[2048]{0:T(1024)}, u32[]{:S(2)}) copy-start(f32[2048]{0:T(1024)} %param.35) | copy-start | bytes 24580
  160.7 34.8 %copy-start.8 = (f32[2048]{0:T(1024)S(1)}, f32[2048]{0:T(1024)}, u32[]{:S(2)}) copy-start(f32[2048]{0:T(1024)} %param.36) | copy-start | bytes 24580
  160.7 34.8 %all-to-all-start.2 = ((bf16[128,16,512]{2,1,0:T(8,128)(2,1)}), bf16[128,16,512]{2,1,0:T(8,128)(2,1)S(1)}, u32[]{:S(2)}, u32[]{:S(2)}) async-start(bf16[128,16,512]{2,1,0:T(8,128)(2,1)} %bitcast.15), calls=%async_computation.2 | async-start | bytes 4194304 | tf_op jit(solution)/shard_map/all_to_all | solution.py:731

commit v3 on v2

--- a/solution.py
+++ b/solution.py
@@ -113,7 +113,7 @@
 def query_kernel(index_ref, *refs):
     query_hbms = refs[:SHARE]
     (
-        gain_hbm, table_hbm, out_hbm, out_ref, gain_ref, table_ref, query_refs, out_sems, in_sems,
+        gain_hbm, table_hbm, out_ref, gain_ref, table_ref, query_refs, in_sems,
     ) = refs[SHARE:]
     arriving = [
         pltpu.make_async_copy(query_hbm, query_refs.at[i], in_sems.at[2 + i])
@@ -149,37 +149,22 @@
             values = query_ref[:tok_rows, h * HEAD : (h + 1) * HEAD].astype(f32)
             out_ref[h, rows, :HEAD] = normed_rotated(values, gain_ref[...], cosine, sine)
             out_ref[h, rows, HEAD:] = apart
-    leaving = [
-        pltpu.make_async_copy(out_ref.at[h], out_hbm.at[h], out_sems.at[h])
-        for h in range(out_ref.shape[0])
-    ]
-    for copy in leaving:
-        copy.start()
-    for copy in leaving:
-        copy.wait()
-
-
-def attention_kernel(query_gain_ref, key_gain_ref, query_hbm, *refs):
+
+
+def attention_kernel(query_gain_ref, key_gain_ref, query_ref, *refs):
     kv_refs = refs[:SHARDS]
     refs = refs[SHARDS:]
     (
-        out_ref, keys_ref, values_ref, first_ref, last_ref, order_ref, small_ref, acc_ref, total_ref, max_ref,
-        tiles_ref, tile_sems, key_sems, value_sems,
+        partner_ref, own_ref, keys_ref, values_ref, first_ref, last_ref, order_ref, small_ref, acc_ref, total_ref, max_ref,
+        key_sems, value_sems,
     ) = refs
-    heads, all_rows, depth = query_hbm.shape
+    heads, all_rows, depth = query_ref.shape
     tok_rows = keys_ref.shape[2]
     rows = acc_ref.shape[0]
     tile = rows // heads
     marked = HEAD + MARKS
     groups = tok_rows // HEAD
     step = pl.program_id(0)
-    steps = all_rows // tile
-    tiles = [
-        pltpu.make_async_copy(
-            query_hbm.at[:, pl.ds(i * tile, tile), :], tiles_ref.at[i], tile_sems.at[i]
-        )
-        for i in range(steps)
-    ]
 
     @pl.when(step == 0)
     def fetch():
@@ -190,7 +175,6 @@
                     kv_ref.at[pl.ds(0, marked)], keys_ref.at[j, pl.ds(0, marked)], key_sems.at[j]
                 )
             )
-        tiles_first = tiles[:1]
         for j, kv_ref in enumerate(kv_refs):
             for g in range(groups):
                 arriving.append(
@@ -200,7 +184,7 @@
                         value_sems.at[j * groups + g],
                     )
                 )
-        for copy in tiles_first + arriving + tiles[1:]:
+        for copy in arriving:
             copy.start()
         largest = jnp.max(jnp.abs(query_gain_ref[...])) * jnp.max(jnp.abs(key_gain_ref[...]))
         small_ref[0] = (largest * (HEAD * score_scale * 1.02) < 50.0).astype(jnp.int32)
@@ -213,9 +197,6 @@
             first_ref[j] = line[MARKS - 1, 0].astype(jnp.int32)
             last_ref[j] = line[MARKS - 1, tok_rows - 1].astype(jnp.int32)
 
-    for i in range(steps):
-        pl.when(step == i)(tiles[i].wait)
-    query_ref = tiles_ref.at[step]
     queries = query_ref[...].reshape(rows, depth)
     low = jnp.int32(1 << 20)
     high = jnp.int32(-1)
@@ -290,8 +271,10 @@
     eye = lax.broadcasted_iota(jnp.int32, (rows_out, LANES), 0) == lax.broadcasted_iota(
         jnp.int32, (rows_out, LANES), 1
     )
+    blocks = tile // rows_out
     for h in range(heads):
-        for i in range(tile // rows_out):
+        for i in range(blocks):
+            out_ref = partner_ref.at[i] if i < blocks // 2 else own_ref.at[i - blocks // 2]
             mine = slice(h * tile + i * rows_out, h * tile + (i + 1) * rows_out)
             lanes = slice(h * HEAD, (h + 1) * HEAD)
             total = jnp.sum(total_ref[mine], axis=1, keepdims=True)
@@ -300,13 +283,13 @@
             level = jnp.where(some, max_ref[mine] + jnp.log2(kept), -1e30)
             share = 1.0 / kept
             mixed = acc_ref[mine] * share
-            out_ref[i, :rows_out, lanes] = mixed.astype(bf16)
+            out_ref[:rows_out, lanes] = mixed.astype(bf16)
             flat = jnp.sum(jnp.where(eye, level, 0.0), axis=0, keepdims=True)
             top = flat.astype(bf16).astype(f32)
             rest = flat - top
             middle = rest.astype(bf16).astype(f32)
             final = rest - middle
-            out_ref[i, rows_out:, lanes] = jnp.concatenate(
+            out_ref[rows_out:, lanes] = jnp.concatenate(
                 [top, middle, final, jnp.zeros((13, LANES), f32)], axis=0
             ).astype(bf16)
 
@@ -491,8 +474,8 @@
     rows = LANES
     heads = out_ref.shape[2] // HEAD
     arriving = [
-        pltpu.make_async_copy(own_any.at[pl.ds(blocks, blocks)], own_ref, sems.at[0]),
-        pltpu.make_async_copy(other_any.at[pl.ds(0, blocks)], other_ref, sems.at[1]),
+        pltpu.make_async_copy(own_any, own_ref, sems.at[0]),
+        pltpu.make_async_copy(other_any, other_ref, sems.at[1]),
     ]
     for copy in arriving:
         copy.start()
@@ -540,13 +523,14 @@
     tile = TILE
     width = heads * HEAD
     steps = all_rows // tile
-    out_block = pl.BlockSpec((tile // LANES, LANES + 16, width), lambda i: (i, 0, 0))
+    half_shape = (tile // LANES // 2, LANES + 16, width)
+    half_block = pl.BlockSpec(half_shape, lambda i: (0, 0, 0))
     return pl.pallas_call(
         attention_kernel,
         grid=(steps,),
-        out_shape=pltpu.HBM((all_rows // LANES, LANES + 16, width), bf16),
-        in_specs=[whole_vmem(), whole_vmem(), in_hbm()] + [pl.BlockSpec(memory_space=pl.ANY)] * SHARDS,
-        out_specs=out_block,
+        out_shape=(pltpu.HBM(half_shape, bf16), pltpu.HBM(half_shape, bf16)),
+        in_specs=[whole_vmem(), whole_vmem(), whole_vmem()] + [pl.BlockSpec(memory_space=pl.ANY)] * SHARDS,
+        out_specs=(half_block, half_block),
         scratch_shapes=[
             pltpu.VMEM((SHARDS, depth, tok_rows), bf16),
             pltpu.VMEM((SHARDS, tok_rows, HEAD), bf16),
@@ -557,15 +541,13 @@
             pltpu.VMEM((heads * tile, HEAD), f32),
             pltpu.VMEM((heads * tile, HEAD), f32),
             pltpu.VMEM((heads * tile, HEAD), f32),
-            pltpu.VMEM((steps, heads, tile, depth), bf16),
-            pltpu.SemaphoreType.DMA((steps,)),
             pltpu.SemaphoreType.DMA((SHARDS,)),
             pltpu.SemaphoreType.DMA((SHARDS * tok_rows // HEAD,)),
         ],
         compiler_params=params(40, 1),
         name="document_attention",
     )(
-        query_gain.reshape(1, HEAD), key_gain.reshape(1, HEAD), held(shared_rot), *kv_parts,
+        query_gain.reshape(1, HEAD), key_gain.reshape(1, HEAD), shared_rot, *kv_parts,
     )
 
 
@@ -641,25 +623,22 @@
 
     shared_rot = pl.pallas_call(
         query_kernel,
-        out_shape=pltpu.HBM((heads, SHARE * tok_rows, 2 * HEAD), bf16),
+        out_shape=jax.ShapeDtypeStruct((heads, SHARE * tok_rows, 2 * HEAD), bf16),
         in_specs=[in_smem()] + [pl.BlockSpec(memory_space=pl.ANY)] * SHARE + [in_hbm()] * 2,
-        out_specs=in_hbm(),
+        out_specs=whole_vmem(),
         scratch_shapes=[
-            pltpu.VMEM((heads, SHARE * tok_rows, 2 * HEAD), bf16),
             pltpu.VMEM((1, HEAD), f32),
             pltpu.VMEM(table.shape, f32),
             pltpu.VMEM((SHARE,) + marked.shape, bf16),
-            pltpu.SemaphoreType.DMA((heads,)),
             pltpu.SemaphoreType.DMA((2 + SHARE,)),
         ],
         compiler_params=params(24),
         name="query_rotation",
     )(index, held(marked), *shared[1:], held(query_gain.reshape(1, HEAD)), held(table))
 
-    partial = attention_call(query_gain, key_gain, shared_rot, kv_parts)
-    other = lax.ppermute(partial, "sp", [(i, i ^ 1) for i in range(sp_size)])
-    blocks = partial.shape[0] // 2
-    block = (blocks,) + partial.shape[1:]
+    partner, own = attention_call(query_gain, key_gain, shared_rot, kv_parts)
+    other = lax.ppermute(partner, "sp", [(i, i ^ 1) for i in range(sp_size)])
+    block = own.shape
     partial = pl.pallas_call(
         merge_kernel,
         out_shape=pltpu.HBM(block, bf16),
@@ -671,7 +650,7 @@
         ],
         compiler_params=params(16),
         name="merge_parts",
-    )(held(partial), other)
+    )(held(own), other)
     partial = lax.all_to_all(
         partial, ("sp", "tp"), 0, 0, tiled=True, axis_index_groups=owner_groups
     )

time: 198 us -> 198 us (level)
  transfers between devices with their start and end apart: 13 -> 13, of which waited for: 7 -> 8; matrix products, arithmetic and copies ran while one was open for 0% -> 0% of each run, Pallas kernels for 2% -> 1%
where the time goes in v3:
time: 198 us
  Pallas kernels  62.7 us (32%)
  waiting for transfers between devices  57.2 us (29%)
  blocking collectives  42.8 us (22%)
  starting transfers between devices  34.1 us (17%)
    all_to_all x1, blocking collectives, per_device(): lax.all_to_all(outbound.reshape(expert_total, CAPACITY * PARTS, cut), ('s...  42.8 us
    pallas_call x1, Pallas kernels, attention_call(): pl.pallas_call(attention_kernel, grid=(steps,), out_shape=(pltpu.HBM(half...  41.5 us
    all_to_all x1, waiting for transfers between devices, per_device(): lax.all_to_all(served.reshape(expert_total, CAPACITY * PARTS, cut), ('sp'...  30.8 us
    ppermute x7, starting transfers between devices, moved(): return lax.ppermute(array, 'sp', pairs)  15.7 us
    all_to_all x1, waiting for transfers between devices, per_device(): lax.all_to_all(partial, ('sp', 'tp'), 0, 0, tiled=True, axis_index_groups...  10.6 us
    ppermute x1, starting transfers between devices, per_device(): other = lax.ppermute(partner, 'sp', [(i, i ^ 1) for i in range(sp_size)])  8.99 us
    ppermute x7, waiting for transfers between devices, moved(): return lax.ppermute(array, 'sp', pairs)  7.02 us
    pallas_call x1, Pallas kernels, per_device(): pl.pallas_call(expert_kernel, out_shape=jax.ShapeDtypeStruct((exchange_ro...  5.93 us
  transfers between devices with their start and end apart: 13, of which 8 were waited for; matrix products, arithmetic and copies ran while one was open for 0% of the time, Pallas kernels for 1%

profile of v3, /device:TPU:1, one launch (start us, length us, event | category | flops | bytes accessed | tf_op | source)
XLA Modules:
  0.0 197.7 jit_solution(16504645293988619462)
XLA Ops:
  0.0 0.0 copy-start.10
  0.0 2.3 %key_rotation.1 = (bf16[272,512]{1,0:T(8,128)(2,1)}, bf16[528,256]{1,0:T(8,128)(2,1)}) custom-call(s32[1]{0:T(128)} %bitcast.2.index_ref, bf16[512,128]{1,0:T(8,128)(2,1)} %key_hbm.1, bf16[512,128]{1,0:T(8,128)(2,1)} %value_hbm.1, s32[1,512]{1,0:T(1,128)} %bitcast.46, f32[1,128]{1,0:T(1,128)} %bitcast.41, f32[640,128]{1,0:T(8,128)} %constant.12.clone.table_hbm.refs_5_, ...), custom_call_target="tpu_custom_call" | custom-call | tf_op jit(solution)/shard_map/key_rotation/pallas_call | solution.py:573
  2.3 0.0 copy-start.4
  2.4 3.8 %collective-permute-start.5 = (bf16[272,512]{1,0:T(8,128)(2,1)}, bf16[272,512]{1,0:T(8,128)(2,1)S(1)}, u32[]{:S(2)}, u32[]{:S(2)}) collective-permute-start(bf16[272,512]{1,0:T(8,128)(2,1)} %get-tuple-element.12.refs_0_), channel_id=1, source_target_pairs={{0,16},{4,20},{8,24},{12,28},{16,0},{20,4},{24,8},{28,12},{32,48},... | collective-permute-start | bytes 835592 | tf_op jit(solution)/shard_map/ppermute | solution.py:607
  6.2 3.8 %collective-permute-start.3 = (bf16[272,512]{1,0:T(8,128)(2,1)}, bf16[272,512]{1,0:T(8,128)(2,1)S(1)}, u32[]{:S(2)}, u32[]{:S(2)}) collective-permute-start(bf16[272,512]{1,0:T(8,128)(2,1)} %get-tuple-element.12.refs_0_), channel_id=1, source_target_pairs={{0,32},{4,100},{8,40},{12,108},{16,48},{20,116},{24,56},{28,124},{... | collective-permute-start | bytes 835592 | tf_op jit(solution)/shard_map/ppermute | solution.py:607
  9.9 2.6 %collective-permute-done.5.refs_3_ = bf16[272,512]{1,0:T(8,128)(2,1)S(1)} collective-permute-done((bf16[272,512]{1,0:T(8,128)(2,1)}, bf16[272,512]{1,0:T(8,128)(2,1)S(1)}, u32[]{:S(2)}, u32[]{:S(2)}) %collective-permute-start.5) | collective-permute-done | bytes 278560 | tf_op jit(solution)/shard_map/ppermute | solution.py:607
  12.5 3.7 %collective-permute-start.7 = (bf16[272,512]{1,0:T(8,128)(2,1)S(1)}, bf16[272,512]{1,0:T(8,128)(2,1)S(1)}, u32[]{:S(2)}, u32[]{:S(2)}) collective-permute-start(bf16[272,512]{1,0:T(8,128)(2,1)S(1)} %collective-permute-done.5.refs_3_), channel_id=1, source_target_pairs={{0,32},{4,100},{8,40},{12,108},{16,48},{20,116},{24,56},{28,124},{... | collective-permute-start | bytes 835592 | tf_op jit(solution)/shard_map/ppermute | solution.py:607
  16.3 1.3 collective-permute-start.1
  17.6 0.0 collective-permute-start
  17.6 1.6 collective-permute-start.4
  19.2 5.7 %collective-permute-done.1.refs_2_ = bf16[528,256]{1,0:T(8,128)(2,1)S(1)} collective-permute-done((bf16[528,256]{1,0:T(8,128)(2,1)}, bf16[528,256]{1,0:T(8,128)(2,1)S(1)}, u32[]{:S(2)}, u32[]{:S(2)}) %collective-permute-start.1) | collective-permute-done | bytes 270368 | tf_op jit(solution)/shard_map/ppermute | solution.py:618
  24.8 0.0 collective-permute-start.8
  24.8 0.0 collective-permute-done.3.refs_1_
  24.8 2.7 %collective-permute-start.6 = (bf16[272,512]{1,0:T(8,128)(2,1)S(1)}, bf16[272,512]{1,0:T(8,128)(2,1)S(1)}, u32[]{:S(2)}, u32[]{:S(2)}) collective-permute-start(bf16[272,512]{1,0:T(8,128)(2,1)S(1)} %collective-permute-done.3.refs_1_), channel_id=1, source_target_pairs={{0,32},{4,100},{8,40},{12,108},{16,48},{20,116},{24,56},{28,124},{... | collective-permute-start | bytes 835592 | tf_op jit(solution)/shard_map/ppermute | solution.py:607
  27.5 0.0 collective-permute-done.7.refs_5_
  27.5 0.1 collective-permute-start.9
  27.6 0.0 collective-permute-done.refs_1_
  27.6 0.0 collective-permute-start.2
  27.6 1.5 collective-permute-done.2.refs_3_
  29.1 2.9 %query_rotation.1.query_ref = bf16[2,2048,256]{2,1,0:T(8,128)(2,1)S(1)} custom-call(s32[1]{0:T(128)} %bitcast.2.index_ref, bf16[528,256]{1,0:T(8,128)(2,1)} %get-tuple-element.11.refs_0_, bf16[528,256]{1,0:T(8,128)(2,1)S(1)} %collective-permute-done.refs_1_, bf16[528,256]{1,0:T(8,128)(2,1)S(1)} %collective-permute-done.1.refs_2_, ...), custom_call_target="tpu_custom_call" | custom-call | tf_op jit(solution)/shard_map/query_rotation/pallas_call | solution.py:624
  32.1 0.0 copy-start.12
  32.1 0.0 collective-permute-done.4.refs_2_
  32.1 1.2 collective-permute-done.8.refs_6_
  33.3 0.0 collective-permute-done.6.refs_4_
  33.3 3.2 %collective-permute-done.9.refs_7_ = bf16[272,512]{1,0:T(8,128)(2,1)S(1)} collective-permute-done((bf16[272,512]{1,0:T(8,128)(2,1)S(1)}, bf16[272,512]{1,0:T(8,128)(2,1)S(1)}, u32[]{:S(2)}, u32[]{:S(2)}) %collective-permute-start.9) | collective-permute-done | bytes 278560 | tf_op jit(solution)/shard_map/ppermute | solution.py:607
  36.5 0.0 copy-done.10
  36.5 0.0 copy-done.11
  36.5 0.0 copy-done.4
  36.5 41.5 %document_attention.1 = (bf16[8,144,256]{2,1,0:T(8,128)(2,1)}, bf16[8,144,256]{2,1,0:T(8,128)(2,1)}) custom-call(f32[1,128]{1,0:T(1,128)S(1)} %bitcast.40, f32[1,128]{1,0:T(1,128)S(1)} %bitcast.42, bf16[2,2048,256]{2,1,0:T(8,128)(2,1)S(1)} %query_rotation.1.query_ref, bf16[272,512]{1,0:T(8,128)(2,1)S(1)} %copy-done.4, ...), custom_call_target="tpu_custom_call" | custom-call | tf_op jit(solution)/shard_map/document_attention/pallas_call | solution.py:528
  78.0 0.0 copy-start.3
  78.0 0.0 copy-start.5
  78.0 0.0 copy-start.6
  78.0 0.0 copy-start.9
  78.0 9.0 %collective-permute-start.10 = (bf16[8,144,256]{2,1,0:T(8,128)(2,1)}, bf16[8,144,256]{2,1,0:T(8,128)(2,1)S(1)}, u32[]{:S(2)}, u32[]{:S(2)}) collective-permute-start(bf16[8,144,256]{2,1,0:T(8,128)(2,1)} %get-tuple-element.14), channel_id=1, source_target_pairs={{0,4},{4,0},{8,12},{12,8},{16,20},{20,16},{24,28},{28,24},{32,36},... | collective-permute-start | bytes 1769480 | tf_op jit(solution)/shard_map/ppermute | solution.py:640
  87.0 0.0 copy-done.12
  87.0 0.1 copy.33
  87.1 0.1 copy.35
  87.2 1.7 collective-permute-done.10.other_any
  88.9 2.8 %merge_parts.1 = bf16[8,144,256]{2,1,0:T(8,128)(2,1)} custom-call(bf16[8,144,256]{2,1,0:T(8,128)(2,1)} %get-tuple-element.13.own_any, bf16[8,144,256]{2,1,0:T(8,128)(2,1)S(1)} %collective-permute-done.10.other_any), custom_call_target="tpu_custom_call" | custom-call | tf_op jit(solution)/shard_map/merge_parts/pallas_call | solution.py:642
  91.6 4.2 %all-to-all-start = ((bf16[8,144,256]{2,1,0:T(8,128)(2,1)}), bf16[8,144,256]{2,1,0:T(8,128)(2,1)S(1)}, u32[]{:S(2)}, u32[]{:S(2)}) async-start(bf16[8,144,256]{2,1,0:T(8,128)(2,1)} %merge_parts.1), calls=%async_computation | async-start | bytes 1179648 | tf_op jit(solution)/shard_map/all_to_all | solution.py:654
  95.8 0.2 convert_reduce_fusion
  96.0 0.1 copy.36
  96.2 0.1 copy.37
  96.2 10.6 %all-to-all-done.part_ref = bf16[8,144,256]{2,1,0:T(8,128)(2,1)S(1)} async-done(((bf16[8,144,256]{2,1,0:T(8,128)(2,1)}), bf16[8,144,256]{2,1,0:T(8,128)(2,1)S(1)}, u32[]{:S(2)}, u32[]{:S(2)}) %all-to-all-start) | async-done | bytes 589856 | tf_op jit(solution)/shard_map/all_to_all | solution.py:654
  106.8 0.0 copy-done.3
  106.8 0.0 copy-done.5
  106.8 0.0 copy-done.6
  106.8 0.0 copy-done.9
  106.8 0.0 copy-start.2
  106.8 4.8 %middle_stream.1 = (bf16[128,2048]{1,0:T(8,128)(2,1)S(1)}, bf16[2048,512]{1,0:T(8,128)(2,1)S(1)}) custom-call(bf16[8,144,256]{2,1,0:T(8,128)(2,1)S(1)} %all-to-all-done.part_ref, f32[1,1024]{1,0:T(1,128)S(1)} %bitcast.38, bf16[1024,2048]{1,0:T(8,128)(2,1)} %proj_ref.1, bf16[128,2048]{1,0:T(8,128)(2,1)S(1)} %copy-done.3, f32[1,2048]{1,0:T(1,128)S(1)} %bitcast.34, ...), custom_call_target="tpu_custom_call" | custom-call | tf_op jit(solution)/shard_map/middle_stream/pallas_call | solution.py:668
  111.7 0.0 copy-start
  111.7 0.0 copy-start.1
  111.7 42.8 %all_to_all.15 = bf16[128,16,512]{2,1,0:T(8,128)(2,1)S(1)} all-to-all(bf16[128,16,512]{2,1,0:T(8,128)(2,1)S(1)} %bitcast.31), channel_id=1, replica_groups=mesh['sp'=32,'tp'=4] {'sp','tp'}, dimensions={0} | all-to-all | bytes 4194304 | tf_op jit(solution)/shard_map/all_to_all | solution.py:689
  154.5 0.0 copy-done.2
  154.5 0.0 copy-done
  154.5 0.0 copy-done.1
  154.5 5.9 %expert.1 = bf16[2048,512]{1,0:T(8,128)(2,1)} custom-call(bf16[2048,512]{1,0:T(8,128)(2,1)S(1)} %bitcast.26, bf16[2048,512]{1,0:T(8,128)(2,1)S(1)} %bitcast.28, bf16[2048,512]{1,0:T(8,128)(2,1)S(1)} %bitcast.29, bf16[512,2048]{1,0:T(8,128)(2,1)S(1)} %bitcast.30), custom_call_target="tpu_custom_call" | custom-call | tf_op jit(solution)/shard_map/expert/pallas_call | solution.py:693
  160.4 3.9 %all-to-all-start.2 = ((bf16[128,16,512]{2,1,0:T(8,128)(2,1)}), bf16[128,16,512]{2,1,0:T(8,128)(2,1)S(1)}, u32[]{:S(2)}, u32[]{:S(2)}) async-start(bf16[128,16,512]{2,1,0:T(8,128)(2,1)} %bitcast.15), calls=%async_computation.2 | async-start | bytes 4194304 | tf_op jit(solution)/shard_map/all_to_all | solution.py:710
  164.3 0.0 copy-done.13
  164.4 0.1 copy.38.weight_ref
  164.5 30.8 %all-to-all-done.2 = bf16[128,16,512]{2,1,0:T(8,128)(2,1)S(1)} async-done(((bf16[128,16,512]{2,1,0:T(8,128)(2,1)}), bf16[128,16,512]{2,1,0:T(8,128)(2,1)S(1)}, u32[]{:S(2)}, u32[]{:S(2)}) %all-to-all-start.2) | async-done | bytes 2097184 | tf_op jit(solution)/shard_map/all_to_all | solution.py:710
  195.2 0.0 copy-done.7
  195.3 0.0 copy-done.8
  195.3 2.4 %final_stream.1 = bf16[128,2048]{1,0:T(8,128)(2,1)} custom-call(bf16[2048,512]{1,0:T(8,128)(2,1)S(1)} %bitcast.27, s32[128,2]{1,0:T(8,128)S(1)} %bitcast.32, f32[128,2]{1,0:T(8,128)S(1)} %copy.38.weight_ref, bf16[128,2048]{1,0:T(8,128)(2,1)S(1)} %get-tuple-element.16.middle_ref, f32[1,2048]{1,0:T(1,128)S(1)} %bitcast.36, f32[1,2048]{1,0:T(1,128)S(1)} %bitcast.37), custom_call_target="tpu_custom_call" | custom-call | tf_op jit(solution)/shard_map/final_stream/pallas_call | solution.py:713
  (7 shorter events, 0.0 us)
Async XLA Ops:
  0.0 36.5 %copy-start.10 = (f32[128]{0:T(128)S(1)}, f32[128]{0:T(128)}, u32[]{:S(2)}) copy-start(f32[128]{0:T(128)} %param.23) | copy-start | bytes 1540
  0.0 36.5 %copy-start.11 = (f32[128]{0:T(128)S(1)}, f32[128]{0:T(128)}, u32[]{:S(2)}) copy-start(f32[128]{0:T(128)} %param.24) | copy-start | bytes 1540
  2.3 34.2 %copy-start.4 = (bf16[272,512]{1,0:T(8,128)(2,1)S(1)}, bf16[272,512]{1,0:T(8,128)(2,1)}, u32[]{:S(2)}) copy-start(bf16[272,512]{1,0:T(8,128)(2,1)} %get-tuple-element.12.refs_0_) | copy-start | bytes 835588
  2.4 10.2 %collective-permute-start.5 = (bf16[272,512]{1,0:T(8,128)(2,1)}, bf16[272,512]{1,0:T(8,128)(2,1)S(1)}, u32[]{:S(2)}, u32[]{:S(2)}) collective-permute-start(bf16[272,512]{1,0:T(8,128)(2,1)} %get-tuple-element.12.refs_0_), channel_id=1, source_target_pairs={{0,16},{4,20},{8,24},{12,28},{16,0},{20,4},{24,8},{28,12},{32,48},... | collective-permute-start | bytes 835592 | tf_op jit(solution)/shard_map/ppermute | solution.py:607
  6.2 18.7 %collective-permute-start.3 = (bf16[272,512]{1,0:T(8,128)(2,1)}, bf16[272,512]{1,0:T(8,128)(2,1)S(1)}, u32[]{:S(2)}, u32[]{:S(2)}) collective-permute-start(bf16[272,512]{1,0:T(8,128)(2,1)} %get-tuple-element.12.refs_0_), channel_id=1, source_target_pairs={{0,32},{4,100},{8,40},{12,108},{16,48},{20,116},{24,56},{28,124},{... | collective-permute-start | bytes 835592 | tf_op jit(solution)/shard_map/ppermute | solution.py:607
  12.5 15.0 %collective-permute-start.7 = (bf16[272,512]{1,0:T(8,128)(2,1)S(1)}, bf16[272,512]{1,0:T(8,128)(2,1)S(1)}, u32[]{:S(2)}, u32[]{:S(2)}) collective-permute-start(bf16[272,512]{1,0:T(8,128)(2,1)S(1)} %collective-permute-done.5.refs_3_), channel_id=1, source_target_pairs={{0,32},{4,100},{8,40},{12,108},{16,48},{20,116},{24,56},{28,124},{... | collective-permute-start | bytes 835592 | tf_op jit(solution)/shard_map/ppermute | solution.py:607
  16.3 8.6 %collective-permute-start.1 = (bf16[528,256]{1,0:T(8,128)(2,1)}, bf16[528,256]{1,0:T(8,128)(2,1)S(1)}, u32[]{:S(2)}, u32[]{:S(2)}) collective-permute-start(bf16[528,256]{1,0:T(8,128)(2,1)} %get-tuple-element.11.refs_0_), channel_id=1, source_target_pairs={{0,8},{4,12},{8,0},{12,4},{16,24},{20,28},{24,16},{28,20},{32,40},... | collective-permute-start | bytes 811016 | tf_op jit(solution)/shard_map/ppermute | solution.py:618
  17.6 10.0 %collective-permute-start = (bf16[528,256]{1,0:T(8,128)(2,1)}, bf16[528,256]{1,0:T(8,128)(2,1)S(1)}, u32[]{:S(2)}, u32[]{:S(2)}) collective-permute-start(bf16[528,256]{1,0:T(8,128)(2,1)} %get-tuple-element.11.refs_0_), channel_id=1, source_target_pairs={{0,4},{4,0},{8,12},{12,8},{16,20},{20,16},{24,28},{28,24},{32,36},... | collective-permute-start | bytes 811016 | tf_op jit(solution)/shard_map/ppermute | solution.py:621
  17.6 14.5 %collective-permute-start.4 = (bf16[272,512]{1,0:T(8,128)(2,1)}, bf16[272,512]{1,0:T(8,128)(2,1)S(1)}, u32[]{:S(2)}, u32[]{:S(2)}) collective-permute-start(bf16[272,512]{1,0:T(8,128)(2,1)} %get-tuple-element.12.refs_0_), channel_id=1, source_target_pairs={{0,96},{4,36},{8,104},{12,44},{16,112},{20,52},{24,120},{28,60},{3... | collective-permute-start | bytes 835592 | tf_op jit(solution)/shard_map/ppermute | solution.py:607
  24.8 8.5 %collective-permute-start.8 = (bf16[272,512]{1,0:T(8,128)(2,1)S(1)}, bf16[272,512]{1,0:T(8,128)(2,1)S(1)}, u32[]{:S(2)}, u32[]{:S(2)}) collective-permute-start(bf16[272,512]{1,0:T(8,128)(2,1)S(1)} %collective-permute-done.5.refs_3_), channel_id=1, source_target_pairs={{0,96},{4,36},{8,104},{12,44},{16,112},{20,52},{24,120},{28,60},{3... | collective-permute-start | bytes 835592 | tf_op jit(solution)/shard_map/ppermute | solution.py:607
  24.8 8.5 %collective-permute-start.6 = (bf16[272,512]{1,0:T(8,128)(2,1)S(1)}, bf16[272,512]{1,0:T(8,128)(2,1)S(1)}, u32[]{:S(2)}, u32[]{:S(2)}) collective-permute-start(bf16[272,512]{1,0:T(8,128)(2,1)S(1)} %collective-permute-done.3.refs_1_), channel_id=1, source_target_pairs={{0,32},{4,100},{8,40},{12,108},{16,48},{20,116},{24,56},{28,124},{... | collective-permute-start | bytes 835592 | tf_op jit(solution)/shard_map/ppermute | solution.py:607
  27.5 9.0 %collective-permute-start.9 = (bf16[272,512]{1,0:T(8,128)(2,1)S(1)}, bf16[272,512]{1,0:T(8,128)(2,1)S(1)}, u32[]{:S(2)}, u32[]{:S(2)}) collective-permute-start(bf16[272,512]{1,0:T(8,128)(2,1)S(1)} %collective-permute-done.7.refs_5_), channel_id=1, source_target_pairs={{0,32},{4,100},{8,40},{12,108},{16,48},{20,116},{24,56},{28,124},{... | collective-permute-start | bytes 835592 | tf_op jit(solution)/shard_map/ppermute | solution.py:607
  27.6 1.6 collective-permute-start.2
  32.1 55.0 %copy-start.12 = (s32[128,2]{0,1:T(2,128)S(1)}, s32[128,2]{0,1:T(2,128)}, u32[]{:S(2)}) copy-start(s32[128,2]{0,1:T(2,128)} %param.30) | copy-start | bytes 3076
  78.0 28.8 %copy-start.3 = (bf16[128,2048]{1,0:T(8,128)(2,1)S(1)}, bf16[128,2048]{1,0:T(8,128)(2,1)}, u32[]{:S(2)}) copy-start(bf16[128,2048]{1,0:T(8,128)(2,1)} %residual_ref.1) | copy-start | bytes 1572868
  78.0 28.8 %copy-start.5 = (f32[2048]{0:T(1024)S(1)}, f32[2048]{0:T(1024)}, u32[]{:S(2)}) copy-start(f32[2048]{0:T(1024)} %param.28) | copy-start | bytes 24580
  78.0 28.8 %copy-start.6 = (f32[2048]{0:T(1024)S(1)}, f32[2048]{0:T(1024)}, u32[]{:S(2)}) copy-start(f32[2048]{0:T(1024)} %param.29) | copy-start | bytes 24580
  78.0 28.8 %copy-start.9 = (f32[1024]{0:T(1024)S(1)}, f32[1024]{0:T(1024)}, u32[]{:S(2)}) copy-start(f32[1024]{0:T(1024)} %param.25) | copy-start | bytes 12292
  78.0 10.8 %collective-permute-start.10 = (bf16[8,144,256]{2,1,0:T(8,128)(2,1)}, bf16[8,144,256]{2,1,0:T(8,128)(2,1)S(1)}, u32[]{:S(2)}, u32[]{:S(2)}) collective-permute-start(bf16[8,144,256]{2,1,0:T(8,128)(2,1)} %get-tuple-element.14), channel_id=1, source_target_pairs={{0,4},{4,0},{8,12},{12,8},{16,20},{20,16},{24,28},{28,24},{32,36},... | collective-permute-start | bytes 1769480 | tf_op jit(solution)/shard_map/ppermute | solution.py:640
  91.6 15.2 %all-to-all-start = ((bf16[8,144,256]{2,1,0:T(8,128)(2,1)}), bf16[8,144,256]{2,1,0:T(8,128)(2,1)S(1)}, u32[]{:S(2)}, u32[]{:S(2)}) async-start(bf16[8,144,256]{2,1,0:T(8,128)(2,1)} %merge_parts.1), calls=%async_computation | async-start | bytes 1179648 | tf_op jit(solution)/shard_map/all_to_all | solution.py:654
  106.8 47.7 %copy-start.2 = (bf16[1,512,2048]{2,1,0:T(8,128)(2,1)S(1)}, bf16[1,512,2048]{2,1,0:T(8,128)(2,1)}, u32[]{:S(2)}) copy-start(bf16[1,512,2048]{2,1,0:T(8,128)(2,1)} %param.34) | copy-start | bytes 6291460
  111.7 42.8 %copy-start = (bf16[1,2048,512]{2,1,0:T(8,128)(2,1)S(1)}, bf16[1,2048,512]{2,1,0:T(8,128)(2,1)}, u32[]{:S(2)}) copy-start(bf16[1,2048,512]{2,1,0:T(8,128)(2,1)} %param.32) | copy-start | bytes 6291460
  111.7 42.8 %copy-start.1 = (bf16[1,2048,512]{2,1,0:T(8,128)(2,1)S(1)}, bf16[1,2048,512]{2,1,0:T(8,128)(2,1)}, u32[]{:S(2)}) copy-start(bf16[1,2048,512]{2,1,0:T(8,128)(2,1)} %param.33) | copy-start | bytes 6291460
  160.4 3.9 %copy-start.13 = (f32[128,2]{0,1:T(2,128)S(1)}, f32[128,2]{0,1:T(2,128)}, u32[]{:S(2)}) copy-start(f32[128,2]{0,1:T(2,128)} %param.31) | copy-start | bytes 3076
  160.4 34.8 %copy-start.7 = (f32[2048]{0:T(1024)S(1)}, f32[2048]{0:T(1024)}, u32[]{:S(2)}) copy-start(f32[2048]{0:T(1024)} %param.35) | copy-start | bytes 24580
  160.4 34.8 %copy-start.8 = (f32[2048]{0:T(1024)S(1)}, f32[2048]{0:T(1024)}, u32[]{:S(2)}) copy-start(f32[2048]{0:T(1024)} %param.36) | copy-start | bytes 24580
  160.4 34.8 %all-to-all-start.2 = ((bf16[128,16,512]{2,1,0:T(8,128)(2,1)}), bf16[128,16,512]{2,1,0:T(8,128)(2,1)S(1)}, u32[]{:S(2)}, u32[]{:S(2)}) async-start(bf16[128,16,512]{2,1,0:T(8,128)(2,1)} %bitcast.15), calls=%async_computation.2 | async-start | bytes 4194304 | tf_op jit(solution)/shard_map/all_to_all | solution.py:710
